TPU v7x, 32 devices: a whole 2x2x4 slice. The times are simulated.
32 devices in a mesh: sp: 16 (over z, y, x), tp: 2 (over core).
Axes of the slice: x: 2, y: 2, z: 4, core: 2. Of those that a mesh axis runs over, the one named last changes fastest.
Arguments:
- tokens: bfloat16 [4096, 2048], P(('sp', 'tp')), may hold values from -6 to 6
- mix_gain: float32 [2048], replicated, may hold values from 0.1 to 1.9
- query_proj: bfloat16 [2048, 1536], P(None, 'tp'), may hold values from -4 to 4
- compressed_projection: bfloat16 [2048, 256], replicated, may hold values from -0.125 to 0.125
- compressed_norm_gain: float32 [256], replicated, may hold values from 0.1 to 1.9
- rope_proj: bfloat16 [2048, 64], replicated, may hold values from -0.125 to 0.125
- key_up: bfloat16 [256, 1024], P(None, 'tp'), may hold values from -4 to 4
- value_up_weight: bfloat16 [256, 1024], P(None, 'tp'), may hold values from -0.375 to 0.375
- scan_input: bfloat16 [2048, 2048], P('sp', 'tp'), may hold values from -0.125 to 0.125
- scan_gate: bfloat16 [2048, 2048], P('sp', 'tp'), may hold values from -0.125 to 0.125
- scan_write: bfloat16 [2048, 1024], P('sp', 'tp'), may hold values from -0.125 to 0.125
- scan_read: bfloat16 [2048, 1024], P('sp', 'tp'), may hold values from -0.125 to 0.125
- step_proj: bfloat16 [2048, 32], replicated, may hold values from -0.125 to 0.125
- conv_input: bfloat16 [4, 2048], P(None, 'tp'), may hold values from -3 to 3
- conv_write: bfloat16 [4, 1024], P(None, 'tp'), may hold values from -3 to 3
- conv_read: bfloat16 [4, 1024], P(None, 'tp'), may hold values from -3 to 3
- decay_log: float32 [32], P('tp'), may hold values from -16 to -2.8
- decay_offset: float32 [4096, 32], P('sp', 'tp'), may hold values from -2.2 to 0
- skip_gain: float32 [32], P('tp'), may hold values from 0.1 to 1.9
- group_gain: float32 [2048], P('tp'), may hold values from 0.1 to 1.9
Outputs:
- attended: bfloat16 [4096, 1024], P('sp', 'tp')
- scanned: bfloat16 [4096, 2048], P('sp', 'tp')
All inputs are finite; a program needn't handle non-finite values.
Results may differ from a plain program's by a relative error of at most 0.017.
The roundings to bfloat16 on the way count: a program that leaves them out, or rounds other values in their place, can miss the bound.
Values may be sent and summed in bfloat16 or wider, within the bound.
No kernel may reach another device: no remote copies, remote signals or barrier semaphores. Data moves between devices by JAX's collectives and lax.ppermute only.
A program may use at most 128 MiB of HBM per device.

v0:
```python
import functools
import math

import jax
import jax.numpy as jnp
from jax import lax
from jax.experimental import pallas as pl
from jax.experimental.pallas import tpu as pltpu
from jax.sharding import Mesh
from jax.sharding import PartitionSpec as P


UNROTATED_WIDTH = 128
ROPE = 64
VALUE_WIDTH = 128
SSM_DIM = 64
SSM_STATE = 128

eps = 1e-06
theta = 10000.0
floor_score = -1e30
LANES = 128
DIRECT = 8


f32 = jnp.float32
bf16 = jnp.bfloat16


def vmem():
    return pl.BlockSpec(memory_space=pltpu.VMEM)


def smem():
    return pl.BlockSpec(memory_space=pltpu.SMEM)


def hbm():
    return pl.BlockSpec(memory_space=pl.ANY)


def nt(a, b):
    return lax.dot_general(a, b, (((1,), (1,)), ((), ())), preferred_element_type=f32)


def tn(a, b):
    return lax.dot_general(a, b, (((0,), (0,)), ((), ())), preferred_element_type=f32)


def nn(a, b, precision=None):
    return lax.dot_general(
        a, b, (((1,), (0,)), ((), ())), precision=precision, preferred_element_type=f32
    )


def exchange(value, axis):
    count = lax.axis_size(axis)
    if count == 1:
        return [value]
    assert count & (count - 1) == 0
    if count <= DIRECT:
        return [value] + [across(value, axis, k) for k in range(1, count)]
    everything = lax.all_gather(value, axis)
    here = lax.axis_index(axis)
    return [
        lax.dynamic_index_in_dim(everything, here ^ k, 0, keepdims=False) for k in range(count)
    ]


def across(value, axis, k):
    count = lax.axis_size(axis)
    return lax.ppermute(value, axis, [(i, i ^ k) for i in range(count)])


def ring(value, axis):
    count = lax.axis_size(axis)
    if count <= DIRECT:
        pieces = [value]
        for _ in range(1, count):
            pairs = [(i, (i + 1) % count) for i in range(count)]
            pieces.append(lax.ppermute(pieces[-1], axis, pairs))
        return pieces
    everything = lax.all_gather(value, axis)
    here = lax.axis_index(axis)
    return [
        lax.dynamic_index_in_dim(everything, (here - k) % count, 0, keepdims=False)
        for k in range(count)
    ]


def three_parts(values):
    high = lax.reduce_precision(values, 8, 7)
    rest = values - high
    middle = lax.reduce_precision(rest, 8, 7)
    return jnp.stack([high, middle, rest - middle]).astype(bf16)


def prologue_kernel(
    where_ref, tokens_ref, mix_ref, proj_ref, gain_ref, rope_ref, step_ref, cos_ref, sin_ref, rows_ref, key_ref
):
    tokens = tokens_ref[...].astype(f32)
    scale = lax.rsqrt(jnp.mean(tokens * tokens, axis=-1, keepdims=True) + eps)
    x = (tokens * scale * mix_ref[...]).astype(bf16)
    model = x.shape[1]
    rows_ref[:, :model] = x
    wide = nn(x, proj_ref[...])
    scale = lax.rsqrt(jnp.mean(wide * wide, axis=-1, keepdims=True) + eps)
    width = wide.shape[1]
    key_ref[:, :width] = (wide * scale * gain_ref[...]).astype(bf16)
    turn = nt(x, rope_ref[...])
    rope = turn.shape[1]
    half = rope // 2
    row = lax.broadcasted_iota(jnp.int32, (rope, 2 * rope), 0)
    col = lax.broadcasted_iota(jnp.int32, (rope, 2 * rope), 1) % rope
    same = (row == col).astype(f32)
    swap = (row == (col + half) % rope).astype(f32)
    best = lax.Precision.HIGHEST
    count = x.shape[0]
    here = pl.ds(pl.multiple_of(where_ref[2] * count, count), count)
    turned = nn(turn, same, best) * cos_ref[here, :] + nn(turn, swap, best) * sin_ref[here, :]
    key_ref[:, width:] = turned.astype(bf16)
    step = jax.nn.softplus(nt(x, step_ref[...]))
    count = step.shape[1]
    row = lax.broadcasted_iota(jnp.int32, (count, LANES), 0)
    col = lax.broadcasted_iota(jnp.int32, (count, LANES), 1)
    tail = jnp.zeros((x.shape[0], LANES), f32)
    for part in range(3):
        piece = step.astype(bf16)
        step = step - piece.astype(f32)
        tail = tail + nn(piece, (col == row + part * count).astype(f32).astype(bf16))
    rows_ref[:, model:] = tail.astype(bf16)


def query_kernel(where_ref, *refs, count, heads):
    pieces = refs[:count]
    w_ref, cos_ref, sin_ref, plain_ref, turned_ref = refs[count:]
    rows = pieces[0].shape[0]
    w = w_ref[...]
    lane = lax.broadcasted_iota(jnp.int32, (rows, LANES), 1)
    low = lane < ROPE
    first = lane % ROPE < ROPE // 2
    for k in range(count):
        start = pl.multiple_of((where_ref[2] ^ k) * rows, rows)
        here = pl.ds(start, rows)
        q = nn(pieces[k][:, : w.shape[0]], w).astype(bf16).astype(f32)
        cos = cos_ref[here, :]
        sin = sin_ref[here, :]
        for pair in range(heads // 2):
            base = pair * 3 * LANES
            t0 = q[:, base : base + LANES]
            t1 = q[:, base + LANES : base + 2 * LANES]
            t2 = q[:, base + 2 * LANES : base + 3 * LANES]
            odd = jnp.where(low, pltpu.roll(t1, ROPE, 1), pltpu.roll(t2, ROPE, 1))
            turn = jnp.where(low, t1, t2)
            other = jnp.where(
                first, pltpu.roll(turn, LANES - ROPE // 2, 1), pltpu.roll(turn, ROPE // 2, 1)
            )
            turned = turn * cos + other * sin
            at = pair * 2 * LANES
            plain_ref[here, at : at + LANES] = t0.astype(bf16)
            plain_ref[here, at + LANES : at + 2 * LANES] = odd.astype(bf16)
            turned_ref[here, pair * LANES : (pair + 1) * LANES] = turned.astype(bf16)


def attention_kernel(
    where_ref,
    plain_ref,
    turned_ref,
    ku_ref,
    vu_ref,
    *refs,
    planes,
    cores,
    slots,
    heads,
    lower,
    upper,
    final,
):
    arrays = planes * cores
    pieces = refs[:arrays]
    refs = refs[arrays:]
    if lower > 0:
        before, refs = refs[:3], refs[3:]
    if final:
        out_ref, top_s, sum_s, acc_s, keys, q_s, sems = refs
    else:
        top_s, sum_s, acc_s, keys, q_s, sems = refs
    length = plain_ref.shape[0]
    rows = length // cores
    width = ku_ref.shape[0]
    ia, ib, it = where_ref[0], where_ref[1], where_ref[2]
    here = ia * planes + ib
    last = jnp.minimum(here + 1, upper)
    factor = (UNROTATED_WIDTH + ROPE) ** -0.5 * math.log2(math.e)

    for k in range(planes):
        for t in range(cores):
            for z in range(slots):
                block = (ia ^ z) * planes + (ib ^ k)

                @pl.when((block >= lower) & (block < last))
                def _():
                    start = pl.multiple_of((block - lower) * length + (it ^ t) * rows, rows)
                    pltpu.make_async_copy(
                        pieces[k * cores + t].at[pl.ds(z * rows, rows), :],
                        keys.at[pl.ds(start, rows), :],
                        sems.at[block - lower],
                    ).start()

    lane = lax.broadcasted_iota(jnp.int32, (length, LANES), 1)
    for h in range(heads):
        q_s[h, :, :LANES] = plain_ref[:, h * LANES : (h + 1) * LANES]
        turned = turned_ref[:, (h // 2) * LANES : (h // 2 + 1) * LANES]
        keep = lane < ROPE if h % 2 == 0 else lane >= ROPE
        q_s[h, :, LANES:] = jnp.where(keep, turned, jnp.zeros_like(turned))
    if lower > 0:
        top_s[...] = before[0][...]
        sum_s[...] = before[1][...]
        acc_s[...] = before[2][...]
    else:
        top_s[...] = jnp.full(top_s.shape, floor_score, f32)
        sum_s[...] = jnp.zeros(sum_s.shape, f32)
        acc_s[...] = jnp.zeros(acc_s.shape, f32)

    def visit(block, masked):
        at = pl.ds(pl.multiple_of((block - lower) * length, length), length)
        pltpu.make_async_copy(keys.at[at, :], keys.at[at, :], sems.at[block - lower]).wait()
        latent = keys[at, :width]
        shared = keys[at, width:]
        key_plain = nn(latent, ku_ref[...]).astype(bf16)
        values = nt(vu_ref[...], latent).astype(bf16)
        if masked:
            key_at = lax.broadcasted_iota(jnp.int32, (length, length), 0)
            query_at = lax.broadcasted_iota(jnp.int32, (length, length), 1)
            seen = key_at <= query_at
        for h in range(heads):
            key = jnp.concatenate([key_plain[:, h * LANES : (h + 1) * LANES], shared], axis=1)
            score = nt(key, q_s[h])
            if masked:
                score = jnp.where(seen, score, -jnp.inf)
            old = top_s[h]
            top = jnp.maximum(old, jnp.max(score, axis=0, keepdims=True))
            weight = jnp.exp2((score - top) * factor)
            shrink = jnp.exp2((old - top) * factor)
            top_s[h] = top
            sum_s[h] = sum_s[h] * shrink + jnp.sum(weight, axis=0, keepdims=True)
            acc_s[h] = acc_s[h] * shrink + nn(
                values[h * VALUE_WIDTH : (h + 1) * VALUE_WIDTH, :], weight.astype(bf16)
            )

    def body(block, carry):
        visit(block, False)
        return carry

    lax.fori_loop(lower, jnp.minimum(here, upper), body, 0)

    @pl.when((here >= lower) & (here < upper))
    def _():
        visit(here, True)

    if final:
        for h in range(heads):
            result = (acc_s[h] / sum_s[h]).T
            out_ref[:, h * VALUE_WIDTH : (h + 1) * VALUE_WIDTH] = result.astype(bf16)


def wide_heads(values, heads, lane):
    tiles = []
    for pair in range(0, heads, 2):
        a = jnp.broadcast_to(values[:, pair : pair + 1], (values.shape[0], LANES))
        b = jnp.broadcast_to(values[:, pair + 1 : pair + 2], (values.shape[0], LANES))
        tiles.append(jnp.where(lane < SSM_DIM, a, b))
    return jnp.concatenate(tiles, axis=1)


def row_copies(where_ref, pieces, parts, target, sems, length, cores, width):
    ib, it = where_ref[1], where_ref[2]
    rows = length // cores
    for piece, (k, t, start, count) in zip(pieces, parts):
        block = ib ^ k
        at = pl.multiple_of(block * length + (it ^ t) * rows + start, count)
        yield pltpu.make_async_copy(
            piece.at[:, pl.ds(0, width)], target.at[pl.ds(at, count), :], sems.at[block]
        )


def weight_copies(where_ref, piece, plane, target, sem, planes):
    depth = piece.shape[0] // planes
    for k in range(planes):
        at = pl.multiple_of((plane * planes + (where_ref[1] ^ k)) * depth, depth)
        yield pltpu.make_async_copy(
            piece.at[pl.ds(k * depth, depth), :], target.at[pl.ds(at, depth), :], sem
        )


def scan_kernel(
    where_ref,
    *refs,
    parts,
    planes,
    cores,
    weights,
    length,
    heads,
    every,
):
    nx = len(parts)
    xs_in = refs[:nx]
    ws_in = refs[nx : nx + weights]
    halo_in = refs[nx + weights : nx + weights + planes * cores]
    (
        extra_ref,
        ci_ref,
        cw_ref,
        cr_ref,
        rate_ref,
        skip_ref,
        mixed_ref,
        reads_ref,
        run_ref,
        state_ref,
        xs,
        ws,
        hs,
        hx,
        pad,
        state_s,
        base_s,
        xsem,
        wsem,
        hsem,
    ) = refs[nx + weights + planes * cores :]
    ia, ib, it = where_ref[0], where_ref[1], where_ref[2]
    deep = ws_in[0].shape[0]
    channels = heads * SSM_DIM
    span = ci_ref.shape[0]
    tiles = hs.shape[0]
    bottom = halo_in[0].shape[0] - tiles
    for k in range(planes):
        for t in range(cores):

            @pl.when(((ib ^ k) == planes - 1) & ((it ^ t) == cores - 1))
            def _():
                pltpu.make_async_copy(
                    halo_in[k * cores + t].at[pl.ds(bottom, tiles), :], hs, hsem
                ).start()

    for k in range(weights):
        for copy in weight_copies(
            where_ref, ws_in[k], (ia - k + weights) % weights, ws, wsem.at[k], planes
        ):
            copy.start()
    for copy in row_copies(where_ref, xs_in, parts, xs, xsem, length, cores, xs.shape[1]):
        copy.start()
    state_s[...] = jnp.zeros(state_s.shape, f32)
    base_s[...] = jnp.zeros(base_s.shape, f32)
    pltpu.make_async_copy(hs, hs, hsem).wait()
    edge = hs[...].astype(f32)
    hx[...] = jnp.zeros(hx.shape, f32)
    for i in range(tiles):
        for r in range(span - 1):
            row = 8 - (span - 1) + r
            hx[row : row + 1, i * LANES : (i + 1) * LANES] = edge[
                i : i + 1, r * LANES : (r + 1) * LANES
            ]
    lane = lax.broadcasted_iota(jnp.int32, (length, LANES), 1)
    li = lax.broadcasted_iota(jnp.int32, (length, length), 0)
    si = lax.broadcasted_iota(jnp.int32, (length, length), 1)
    causal = si <= li
    tril = causal.astype(f32).astype(bf16)
    model = ws.shape[0]
    wide_lane = lax.broadcasted_iota(jnp.int32, (length, channels), 1)

    def onehot(rows, columns, test):
        source = lax.broadcasted_iota(jnp.int32, (rows, columns), 0)
        target = lax.broadcasted_iota(jnp.int32, (rows, columns), 1)
        return test(source, target).astype(f32)

    local = rate_ref.shape[1]
    best = lax.Precision.HIGHEST
    first = it * local + ib * heads
    pick = onehot(
        LANES,
        LANES,
        lambda i, j: (i % every == first + j % heads) & (i < 3 * every) & (j < 3 * heads),
    ).astype(bf16)
    pick_offset = onehot(
        16, LANES, lambda i, j: (i % heads == j % heads) & (i < 3 * heads) & (j < 3 * heads)
    ).astype(bf16)
    pick_rate = onehot(local, LANES, lambda i, j: (i == ib * heads + j % heads) & (j < 3 * heads))
    pick_skip = onehot(local, channels, lambda i, j: i == ib * heads + j // SSM_DIM)
    rate = -jnp.exp(jnp.broadcast_to(rate_ref[...], (8, local)))
    rate = nn(rate, pick_rate, best)[:1]
    skip = nn(jnp.broadcast_to(skip_ref[...], (8, local)), pick_skip, best)[:1]

    def mine(ref, width):
        return ref[:, pl.ds(pl.multiple_of(ib * width, width), width)].astype(f32)

    taps = jnp.concatenate(
        [mine(ci_ref, channels), mine(cw_ref, SSM_STATE), mine(cr_ref, SSM_STATE)], axis=1
    )
    for k in range(weights):
        pltpu.make_async_copy(ws_in[k], ws.at[pl.ds(0, deep), :], wsem.at[k]).wait()
    pad[0:8, :] = nn(hx[...].astype(bf16), ws[...]).astype(bf16).astype(f32)

    def chunk(c, carry):
        here = pl.ds(pl.multiple_of(c * length, length), length)
        pltpu.make_async_copy(xs.at[here, :], xs.at[here, :], xsem.at[c]).wait()
        raw = nn(xs[here, :model], ws[...]).astype(bf16)
        pad[8:, :] = raw.astype(f32)
        total = jnp.zeros(raw.shape, f32)
        for k in range(span):
            total = total + taps[k : k + 1, :] * pad[8 - span + 1 + k : 8 - span + 1 + k + length, :]
        mixed_in = jax.nn.silu(total).astype(bf16)
        pad[0:8, :] = pad[length : length + 8, :]
        head = mixed_in[:, :channels].astype(f32)
        write = mixed_in[:, channels : channels + SSM_STATE]
        read = mixed_in[:, channels + SSM_STATE :]
        reads_ref[here, :] = read
        step = nn(xs[here, model:], pick)
        offset = tn(extra_ref[ib ^ c], pick_offset)
        decay = rate * step + offset
        high = decay.astype(bf16)
        rest = decay - high.astype(f32)
        middle = rest.astype(bf16)
        least = rest - middle.astype(f32)
        split = jnp.where(lane < heads, high.astype(f32), middle.astype(f32))
        split = jnp.where(lane < 2 * heads, split, least).astype(bf16)
        running = nn(tril, split)
        running = (
            running
            + pltpu.roll(running, LANES - heads, 1)
            + pltpu.roll(running, LANES - 2 * heads, 1)
        )
        run_ref[here, :] = running + base_s[...]
        base_s[...] = base_s[...] + running[length - 1 :, :]
        across = running.T
        stepped = head * wide_heads(step, heads, lane)
        inner = nt(read, write)
        reach = jnp.exp(wide_heads(running, heads, lane))
        out = nn(read, state_s[...].astype(bf16)) * reach + skip * head
        for h in range(heads):
            spread = running[:, h : h + 1] - across[h : h + 1, :]
            fading = jnp.exp(jnp.where(causal, spread, floor_score))
            mine = (wide_lane >= h * SSM_DIM) & (wide_lane < (h + 1) * SSM_DIM)
            out = out + nn(
                (inner * fading).astype(bf16), jnp.where(mine, stepped, 0.0).astype(bf16)
            )
        mixed_ref[here, :] = out
        ending = running[length - 1 :, :]
        to_end = jnp.exp(wide_heads(ending - running, heads, lane))
        update = tn(write, (stepped * to_end).astype(bf16))
        state_s[...] = state_s[...] * reach[length - 1 :, :] + update
        return carry

    lax.fori_loop(0, planes, chunk, 0)
    state_ref[: SSM_STATE, :] = state_s[...].astype(bf16)
    total = wide_heads(base_s[...], heads, lane[:1])
    high = total.astype(bf16)
    rest = total - high.astype(f32)
    middle = rest.astype(bf16)
    least = (rest - middle.astype(f32)).astype(bf16)
    tail = jnp.concatenate(
        [high, middle, least, jnp.zeros((SSM_STATE // 8 - 3, channels), bf16)], axis=0
    )
    state_ref[SSM_STATE :, :] = tail


def gate_kernel(where_ref, *refs, parts, planes, cores, weights, length):
    nx = len(parts)
    xs_in = refs[:nx]
    ws_in = refs[nx : nx + weights]
    out_ref, xs, ws, xsem, wsem = refs[nx + weights :]
    ia = where_ref[0]
    deep = ws_in[0].shape[0]
    model = ws.shape[0]

    for k in range(weights):
        for copy in weight_copies(where_ref, ws_in[k], ia ^ k, ws, wsem.at[k], planes):
            copy.start()
    for copy in row_copies(where_ref, xs_in, parts, xs, xsem, length, cores, model):
        copy.start()
    for k in range(weights):
        pltpu.make_async_copy(ws_in[k], ws.at[pl.ds(0, deep), :], wsem.at[k]).wait()
    batch = 2 if planes % 2 == 0 else 1

    def some(c, carry):
        for i in range(batch):
            block = c * batch + i
            at = pl.ds(pl.multiple_of(block * length, length), length)
            pltpu.make_async_copy(xs.at[at, :], xs.at[at, :], xsem.at[block]).wait()
        here = pl.ds(pl.multiple_of(c * batch * length, batch * length), batch * length)
        out_ref[here, :] = jax.nn.silu(nn(xs[here, :], ws[...]).astype(bf16).astype(f32))
        return carry

    lax.fori_loop(0, planes // batch, some, 0)


def finish_kernel(
    where_ref, states_ref, mixed_ref, reads_ref, gate_ref, run_ref, gain_ref, out_ref, into_s, *, heads
):
    here = where_ref[0]
    rows = mixed_ref.shape[0]
    channels = mixed_ref.shape[1]

    @pl.when(pl.program_id(0) == 0)
    def _():
        into_s[...] = jnp.zeros(into_s.shape, f32)

        def add(j, carry):
            piece = states_ref[here ^ j].astype(f32)
            decay = jnp.exp(
                piece[SSM_STATE : SSM_STATE + 1]
                + piece[SSM_STATE + 1 : SSM_STATE + 2]
                + piece[SSM_STATE + 2 : SSM_STATE + 3]
            )
            into_s[...] = into_s[...] * decay + piece[:SSM_STATE]
            return carry

        lax.fori_loop(0, here, add, 0)

    lane = lax.broadcasted_iota(jnp.int32, (rows, LANES), 1)
    reach = jnp.exp(wide_heads(run_ref[...], heads, lane))
    mixed = mixed_ref[...] + nn(reads_ref[...], into_s[...].astype(bf16)) * reach
    gated = mixed * gate_ref[...]
    scale = lax.rsqrt(jnp.mean(gated * gated, axis=-1, keepdims=True) + eps)
    gain = gain_ref[:, pl.ds(pl.multiple_of(where_ref[1] * channels, channels), channels)]
    out_ref[...] = (gated * scale * gain).astype(bf16)


def params():
    return pltpu.CompilerParams(vmem_limit_bytes=60 * 1024 * 1024)


def cost(flops):
    return pl.CostEstimate(flops=flops, bytes_accessed=flops // 1000, transcendentals=0)


def shape(dims, kind):
    return jax.ShapeDtypeStruct(dims, kind)


def shards(
    tokens,
    mix_gain,
    query_proj,
    compressed_projection,
    compressed_norm_gain,
    rope_proj,
    key_up,
    value_up_weight,
    scan_input,
    scan_gate,
    scan_write,
    scan_read,
    step_proj,
    conv_input,
    conv_write,
    conv_read,
    decay_log,
    decay_offset,
    skip_gain,
    group_gain,
):
    A, B, T = lax.axis_size("a"), lax.axis_size("b"), lax.axis_size("tp")
    ia, ib, it = (lax.axis_index(name).astype(jnp.int32) for name in ("a", "b", "tp"))
    where = jnp.stack([ia, ib, it])
    rows, model = tokens.shape
    length = rows * T
    heads = key_up.shape[1] // UNROTATED_WIDTH
    key_width = key_up.shape[0] + 2 * ROPE
    groups = scan_write.shape[1] // SSM_STATE
    local = decay_log.shape[0]
    per_group = local // groups
    channels = per_group * SSM_DIM
    depth = scan_write.shape[0]
    every = step_proj.shape[1]
    taps = conv_input.shape[0]
    span = B * length
    assert groups == B and channels == length
    assert 3 * every <= LANES and 3 * per_group <= 16
    assert (taps - 1) * LANES == key_width

    def regrouped(pieces):
        moved = []
        for k in range(B):
            group = ib ^ k
            parts = [
                lax.dynamic_slice_in_dim(piece, group * width, width, 1)
                for piece, width in pieces
            ]
            value = parts[0] if len(parts) == 1 else jnp.concatenate(parts, axis=1)
            moved.append(across(value, "b", k) if k else value)
        return moved

    positions = (ia * B + ib) * length + jnp.arange(length, dtype=jnp.int32)
    half = ROPE // 2
    freqs = theta ** (-jnp.arange(half, dtype=f32) * 2.0 / ROPE)
    angle = positions.astype(f32)[:, None] * jnp.tile(freqs, LANES // half)[None, :]
    sign = jnp.where(jnp.arange(LANES) % ROPE < half, -1.0, 1.0).astype(f32)
    cosine = jnp.cos(angle)
    sine = jnp.sin(angle) * sign[None, :]

    own, key_own = pl.pallas_call(
        prologue_kernel,
        in_specs=[smem()] + [vmem()] * 8,
        out_shape=(shape((rows, model + LANES), bf16), shape((rows, key_width), bf16)),
        compiler_params=params(),
        cost_estimate=cost(2 * rows * model * 1024),
        name="prologue",
    )(
        where,
        tokens,
        mix_gain.reshape(1, -1),
        compressed_projection,
        compressed_norm_gain.reshape(1, -1),
        rope_proj.T,
        step_proj.T,
        cosine,
        sine,
    )
    scan_input, key_own = lax.optimization_barrier((scan_input, key_own))
    packed = regrouped([(scan_input, channels), (scan_write, SSM_STATE), (scan_read, SSM_STATE)])
    packed = jnp.concatenate(packed, axis=0)

    edge = lax.ppermute(
        own[rows - taps + 1 :, :model], "a", [(i, i + 1) for i in range(A - 1)]
    )
    edge = edge.reshape(taps - 1, model // LANES, LANES)
    edge = jnp.transpose(edge, (1, 0, 2)).reshape(model // LANES, key_width)
    key_stack = jnp.concatenate(exchange(key_own, "a") + [edge], axis=0)
    packed, key_stack = lax.optimization_barrier((packed, key_stack))
    w_pieces = ring(packed, "a")
    key_pieces = []
    for piece in exchange(key_stack, "b"):
        key_pieces += exchange(piece, "tp")

    if B == 4:
        side, front = across(own, "b", 1), across(own, "b", 2)
        some = rows // 2
        far = [across(side[:some], "b", 2), across(front[some:], "b", 1)]
        plane = [(0, 0, own), (1, 0, side), (2, 0, front), (3, 0, far[0]), (3, some, far[1])]
    else:
        plane = [(k, 0, piece) for k, piece in enumerate(exchange(own, "b"))]
    x_pieces = []
    parts = []
    for k, start, piece in plane:
        for t, part in enumerate(exchange(piece, "tp")):
            x_pieces.append(part)
            parts.append((k, t, start, part.shape[0]))

    offsets = three_parts(decay_offset.T).reshape(3, groups, per_group, length)
    offsets = jnp.transpose(offsets, (1, 0, 2, 3)).reshape(groups, 3 * per_group, length)
    offsets = jnp.pad(offsets, ((0, 0), (0, 16 - 3 * per_group), (0, 0)))
    offsets = jnp.transpose(offsets, (1, 0, 2)).reshape(16, groups * length)
    extra = regrouped([(jnp.concatenate([scan_gate, offsets], axis=0), channels)])
    g_pieces = exchange(jnp.concatenate([e[:depth] for e in extra], axis=0), "a")
    tails = jnp.stack([e[depth:] for e in extra])
    value_t = value_up_weight.T

    even = heads + heads % 2
    wq = query_proj
    if even != heads:
        wq = jnp.pad(wq, ((0, 0), (0, UNROTATED_WIDTH + ROPE)))
    plain, turned = pl.pallas_call(
        functools.partial(query_kernel, count=T, heads=even),
        in_specs=[smem()] + [vmem()] * (T + 3),
        out_shape=(shape((length, even * LANES), bf16), shape((length, even // 2 * LANES), bf16)),
        compiler_params=params(),
        cost_estimate=cost(2 * length * model * even * 256),
        name="query",
    )(where, *x_pieces[:T], wq, cosine, sine)

    def attend(place, lower, upper, carry):
        final = upper == A * B
        carried = (
            shape((heads, 1, length), f32),
            shape((heads, 1, length), f32),
            shape((heads, VALUE_WIDTH, length), f32),
        )
        outs = (shape((length, heads * VALUE_WIDTH), bf16),) if final else carried
        scratch = [pltpu.VMEM(c.shape, f32) for c in carried] if final else []
        return pl.pallas_call(
            functools.partial(
                attention_kernel,
                planes=B,
                cores=T,
                slots=A,
                heads=heads,
                lower=lower,
                upper=upper,
                final=final,
            ),
            in_specs=[smem()] + [vmem()] * 4 + [hbm()] * (B * T) + [vmem()] * len(carry),
            out_specs=tuple(vmem() for _ in outs),
            out_shape=outs,
            scratch_shapes=scratch
            + [
                pltpu.VMEM(((upper - lower) * length, key_width), bf16),
                pltpu.VMEM((heads, length, 2 * LANES), bf16),
                pltpu.SemaphoreType.DMA((upper - lower,)),
            ],
            compiler_params=params(),
            cost_estimate=cost(4 * length * (upper - lower) * length * LANES * 8),
            name="attention",
        )(place, plain, turned, key_up, value_t, *key_pieces, *carry)

    first_part = (3 * A * B) // 4
    carry = attend(where, 0, first_part, ())
    then, carry = lax.optimization_barrier((where, carry))

    conv = channels + 2 * SSM_STATE
    mixed, reads, run, state = pl.pallas_call(
        functools.partial(
            scan_kernel,
            parts=tuple(parts),
            planes=B,
            cores=T,
            weights=A,
            length=length,
            heads=per_group,
            every=every,
        ),
        in_specs=[smem()] + [hbm()] * (len(parts) + A + B * T) + [vmem()] * 6,
        out_specs=[vmem()] * 4,
        out_shape=(
            shape((span, channels), f32),
            shape((span, SSM_STATE), bf16),
            shape((span, LANES), f32),
            shape((SSM_STATE + SSM_STATE // 8, channels), bf16),
        ),
        scratch_shapes=[
            pltpu.VMEM((span, model + LANES), bf16),
            pltpu.VMEM((model, conv), bf16),
            pltpu.VMEM((model // LANES, key_width), bf16),
            pltpu.VMEM((8, model), f32),
            pltpu.VMEM((8 + length, conv), f32),
            pltpu.VMEM((SSM_STATE, channels), f32),
            pltpu.VMEM((1, LANES), f32),
            pltpu.SemaphoreType.DMA((B,)),
            pltpu.SemaphoreType.DMA((A,)),
            pltpu.SemaphoreType.DMA,
        ],
        compiler_params=params(),
        cost_estimate=cost(4 * span * model * conv),
        name="state_scan",
    )(
        then,
        *x_pieces,
        *w_pieces,
        *key_pieces,
        tails,
        conv_input,
        conv_write,
        conv_read,
        decay_log.reshape(1, -1),
        skip_gain.reshape(1, -1),
    )

    states = jnp.stack(exchange(state, "a"))
    then, mixed = lax.optimization_barrier((then, mixed))
    gate = pl.pallas_call(
        functools.partial(
            gate_kernel, parts=tuple(parts), planes=B, cores=T, weights=A, length=length
        ),
        in_specs=[smem()] + [hbm()] * (len(parts) + A),
        out_specs=vmem(),
        out_shape=shape((span, channels), f32),
        scratch_shapes=[
            pltpu.VMEM((span, model), bf16),
            pltpu.VMEM((model, channels), bf16),
            pltpu.SemaphoreType.DMA((B,)),
            pltpu.SemaphoreType.DMA((A,)),
        ],
        compiler_params=params(),
        cost_estimate=cost(2 * span * model * channels),
        name="gate",
    )(then, *x_pieces, *g_pieces)

    scanned = pl.pallas_call(
        functools.partial(finish_kernel, heads=per_group),
        grid=(B,),
        in_specs=[
            smem(),
            pl.BlockSpec(states.shape, lambda i: (0, 0, 0)),
            pl.BlockSpec((length, channels), lambda i: (i, 0)),
            pl.BlockSpec((length, SSM_STATE), lambda i: (i, 0)),
            pl.BlockSpec((length, channels), lambda i: (i, 0)),
            pl.BlockSpec((length, LANES), lambda i: (i, 0)),
            pl.BlockSpec((1, group_gain.shape[0]), lambda i: (0, 0)),
        ],
        out_specs=pl.BlockSpec((length, channels), lambda i: (i, 0)),
        out_shape=shape((span, channels), bf16),
        scratch_shapes=[pltpu.VMEM((SSM_STATE, channels), f32)],
        compiler_params=params(),
        name="finish",
    )(where, states, mixed, reads, gate, run, group_gain.reshape(1, -1))
    last, scanned = lax.optimization_barrier((then, scanned))
    (attended,) = attend(last, first_part, A * B, carry)
    if B > 1:
        scanned = lax.all_to_all(scanned.reshape(B, length, channels), "b", 0, 0, tiled=True)
        scanned = jnp.transpose(scanned, (1, 0, 2)).reshape(length, B * channels)
    return (attended, scanned)


def solution(mesh):
    S, T = mesh.shape["sp"], mesh.shape["tp"]
    sp = ("a", "b")
    in_specs = (
        P(("a", "b", "tp"), None),
        P(),
        P(None, "tp"),
        P(),
        P(),
        P(),
        P(None, "tp"),
        P(None, "tp"),
        P(sp, "tp"),
        P(sp, "tp"),
        P(sp, "tp"),
        P(sp, "tp"),
        P(),
        P(None, "tp"),
        P(None, "tp"),
        P(None, "tp"),
        P("tp"),
        P(sp, "tp"),
        P("tp"),
        P("tp"),
    )
    out_specs = (P(sp, "tp"), P(sp, "tp"))

    def run(*arrays):
        B = arrays[10].shape[1] // SSM_STATE // T
        assert S % B == 0
        fine = Mesh(mesh.devices.reshape(S // B, B, T), ("a", "b", "tp"))
        body = jax.shard_map(
            shards, mesh=fine, in_specs=in_specs, out_specs=out_specs, check_vma=False
        )
        return body(*arrays)

    return run
```

profile of v0, /device:TPU:16, one launch (start us, length us, event | category | flops | bytes accessed | tf_op | source)
XLA Modules:
  0.0 157.2 jit_solution(15528792878169795868)
XLA Ops:
  1.4 1.2 fusion
  2.7 3.8 %prologue.1 = (bf16[128,2176]{1,0:T(8,128)(2,1)}, bf16[128,384]{1,0:T(8,128)(2,1)}) custom-call(s32[3]{0:T(128)} %pad_add_fusion.where_ref, bf16[128,2048]{1,0:T(8,128)(2,1)} %tokens_ref.1, f32[1,2048]{1,0:T(1,128)} %bitcast.61, bf16[2048,256]{1,0:T(8,128)(2,1)} %proj_ref.1, f32[1,256]{1,0:T(1,128)} %bitcast.63, bf16[64,2048]{1,0:T(8,128)(2,1)} %bitcast.51, ...), custom_call_target="tpu_custom_call" | custom-call | flops 536870912 | bytes 536870 | tf_op jit(solution)/shard_map/prologue/pallas_call | solution.py:605
  6.5 1.7 %collective-permute-start.4 = (bf16[128,384]{1,0:T(8,128)(2,1)}, bf16[128,384]{1,0:T(8,128)(2,1)S(1)}, u32[]{:S(2)}, u32[]{:S(2)}) collective-permute-start(bf16[128,384]{1,0:T(8,128)(2,1)} %get-tuple-element.30), channel_id=1, source_target_pairs={{0,8},{8,0},{16,24},{24,16},{1,9},{9,1},{17,25},{25,17},{2,10},{10... | collective-permute-start | bytes 294920 | tf_op jit(solution)/shard_map/ppermute | solution.py:72
  8.4 1.6 %collective-permute-start.6 = (bf16[128,384]{1,0:T(8,128)(2,1)}, bf16[128,384]{1,0:T(8,128)(2,1)S(1)}, u32[]{:S(2)}, u32[]{:S(2)}) collective-permute-start(bf16[128,384]{1,0:T(8,128)(2,1)} %get-tuple-element.30), channel_id=1, source_target_pairs={{0,24},{8,16},{16,8},{24,0},{1,25},{9,17},{17,9},{25,1},{2,26},{10... | collective-permute-start | bytes 294920 | tf_op jit(solution)/shard_map/ppermute | solution.py:72
  10.0 1.0 constant_dynamic-slice_fusion.15
  11.1 1.6 collective-permute-start.1
  13.2 0.8 slice.33
  14.3 1.6 %collective-permute-start.2 = (bf16[128,512]{1,0:T(8,128)(2,1)S(1)}, bf16[128,512]{1,0:T(8,128)(2,1)S(1)}, u32[]{:S(2)}, u32[]{:S(2)}) collective-permute-start(bf16[128,512]{1,0:T(8,128)(2,1)S(1)} %pad_maximum_fusion.4), channel_id=1, source_target_pairs={{0,4},{2,6},{4,0},{6,2},{1,5},{3,7},{5,1},{7,3},{8,12},{10,14},{12... | collective-permute-start | bytes 393224 | tf_op jit(solution)/shard_map/ppermute | solution.py:72
  15.9 2.3 %collective-permute-start.3 = (bf16[128,512]{1,0:T(8,128)(2,1)S(1)}, bf16[128,512]{1,0:T(8,128)(2,1)S(1)}, u32[]{:S(2)}, u32[]{:S(2)}) collective-permute-start(bf16[128,512]{1,0:T(8,128)(2,1)S(1)} %pad_maximum_fusion.5), channel_id=1, source_target_pairs={{0,6},{2,4},{4,2},{6,0},{1,7},{3,5},{5,3},{7,1},{8,14},{10,12},{12... | collective-permute-start | bytes 393224 | tf_op jit(solution)/shard_map/ppermute | solution.py:72
  18.8 4.8 %collective-permute-start.7 = (bf16[3,2048]{1,0:T(4,128)(2,1)S(1)}, bf16[3,2048]{1,0:T(4,128)(2,1)S(1)}, u32[]{:S(2)}, u32[]{:S(2)}) collective-permute-start(bf16[3,2048]{1,0:T(4,128)(2,1)S(1)} %slice.33), channel_id=1, source_target_pairs={{0,8},{8,16},{16,24},{1,9},{9,17},{17,25},{2,10},{10,18},{18,26},{... | collective-permute-start | bytes 36872 | tf_op jit(solution)/shard_map/ppermute | solution.py:627
  23.6 1.4 collective-permute-done.7
  25.0 1.8 %collective-permute-start.28 = (bf16[144,256]{1,0:T(8,128)(2,1)S(1)}, bf16[144,256]{1,0:T(8,128)(2,1)}, u32[]{:S(2)}, u32[]{:S(2)}) collective-permute-start(bf16[144,256]{1,0:T(8,128)(2,1)S(1)} %get-tuple-element.49), channel_id=1, source_target_pairs={{0,6},{2,4},{4,2},{6,0},{1,7},{3,5},{5,3},{7,1},{8,14},{10,12},{12... | collective-permute-start | bytes 221192 | tf_op jit(solution)/shard_map/ppermute | solution.py:72
  26.9 5.5 %collective-permute-done.3 = bf16[128,512]{1,0:T(8,128)(2,1)S(1)} collective-permute-done((bf16[128,512]{1,0:T(8,128)(2,1)S(1)}, bf16[128,512]{1,0:T(8,128)(2,1)S(1)}, u32[]{:S(2)}, u32[]{:S(2)}) %collective-permute-start.3) | collective-permute-done | bytes 131104 | tf_op jit(solution)/shard_map/ppermute | solution.py:72
  32.4 1.6 collective-permute-start.9
  34.2 1.8 %collective-permute-start.27 = (bf16[144,256]{1,0:T(8,128)(2,1)S(1)}, bf16[144,256]{1,0:T(8,128)(2,1)}, u32[]{:S(2)}, u32[]{:S(2)}) collective-permute-start(bf16[144,256]{1,0:T(8,128)(2,1)S(1)} %get-tuple-element.50), channel_id=1, source_target_pairs={{0,4},{2,6},{4,0},{6,2},{1,5},{3,7},{5,1},{7,3},{8,12},{10,14},{12... | collective-permute-start | bytes 221192 | tf_op jit(solution)/shard_map/ppermute | solution.py:72
  36.5 8.6 %collective-permute-done.27 = bf16[144,256]{1,0:T(8,128)(2,1)} collective-permute-done((bf16[144,256]{1,0:T(8,128)(2,1)S(1)}, bf16[144,256]{1,0:T(8,128)(2,1)}, u32[]{:S(2)}, u32[]{:S(2)}) %collective-permute-start.27) | collective-permute-done | bytes 73760 | tf_op jit(solution)/shard_map/ppermute | solution.py:72
  45.1 2.5 %collective-permute-start.23 = (bf16[512,512]{1,0:T(8,128)(2,1)S(1)}, bf16[512,512]{1,0:T(8,128)(2,1)}, u32[]{:S(2)}, u32[]{:S(2)}) collective-permute-start(bf16[512,512]{1,0:T(8,128)(2,1)S(1)} %pad_maximum_fusion.refs_10_), channel_id=1, source_target_pairs={{0,8},{8,16},{16,24},{24,0},{1,9},{9,17},{17,25},{25,1},{2,10},{10... | collective-permute-start | bytes 1572872 | tf_op jit(solution)/shard_map/ppermute | solution.py:81
  47.6 1.8 %copy.26 = bf16[256,512]{0,1:T(8,128)(2,1)} copy(bf16[256,512]{1,0:T(8,128)(2,1)} %param.27) | data formatting | bytes 524288 | tf_op args[7]
  49.4 1.9 %collective-permute-start.13 = (bf16[528,384]{1,0:T(8,128)(2,1)S(1)}, bf16[528,384]{1,0:T(8,128)(2,1)}, u32[]{:S(2)}, u32[]{:S(2)}) collective-permute-start(bf16[528,384]{1,0:T(8,128)(2,1)S(1)} %constant_dynamic-update-slice_fusion.refs_0_.refs_14_), channel_id=1, source_target_pairs={{0,6},{2,4},{4,2},{6,0},{1,7},{3,5},{5,3},{7,1},{8,14},{10,12},{12... | collective-permute-start | bytes 1216520 | tf_op jit(solution)/shard_map/ppermute | solution.py:72
  52.0 13.5 %collective-permute-done.17.refs_4_ = bf16[128,2176]{1,0:T(8,128)(2,1)S(1)} collective-permute-done((bf16[128,2176]{1,0:T(8,128)(2,1)S(1)}, bf16[128,2176]{1,0:T(8,128)(2,1)S(1)}, u32[]{:S(2)}, u32[]{:S(2)}) %collective-permute-start.17) | collective-permute-done | bytes 557088 | tf_op jit(solution)/shard_map/ppermute | solution.py:72
  65.5 1.4 collective-permute-start.24
  66.9 0.7 slice_bitcast_fusion
  67.7 1.4 collective-permute-start.21
  69.1 0.7 slice_bitcast_fusion.1
  69.9 2.1 %collective-permute-done.19.refs_6_ = bf16[64,2176]{1,0:T(8,128)(2,1)S(1)} collective-permute-done((bf16[64,2176]{1,0:T(8,128)(2,1)S(1)}, bf16[64,2176]{1,0:T(8,128)(2,1)S(1)}, u32[]{:S(2)}, u32[]{:S(2)}) %collective-permute-start.19) | collective-permute-done | bytes 278560 | tf_op jit(solution)/shard_map/ppermute | solution.py:72
  72.1 4.7 %collective-permute-done.21.refs_8_ = bf16[64,2176]{1,0:T(8,128)(2,1)S(1)} collective-permute-done((bf16[64,2176]{1,0:T(8,128)(2,1)S(1)}, bf16[64,2176]{1,0:T(8,128)(2,1)S(1)}, u32[]{:S(2)}, u32[]{:S(2)}) %collective-permute-start.21) | collective-permute-done | bytes 278560 | tf_op jit(solution)/shard_map/ppermute | solution.py:72
  77.4 1.8 %collective-permute-start.25 = (bf16[512,512]{1,0:T(8,128)(2,1)}, bf16[512,512]{1,0:T(8,128)(2,1)}, u32[]{:S(2)}, u32[]{:S(2)}) collective-permute-start(bf16[512,512]{1,0:T(8,128)(2,1)} %collective-permute-done.24.refs_12_), channel_id=1, source_target_pairs={{0,8},{8,16},{16,24},{24,0},{1,9},{9,17},{17,25},{25,1},{2,10},{10... | collective-permute-start | bytes 1572872 | tf_op jit(solution)/shard_map/ppermute | solution.py:81
  79.2 0.6 pad_maximum_fusion.6.refs_22_
  79.9 0.8 slice.49
  80.7 0.8 slice.50
  81.6 0.8 slice.51
  82.5 4.3 %query.1 = (bf16[256,512]{1,0:T(8,128)(2,1)}, bf16[256,256]{1,0:T(8,128)(2,1)}) custom-call(s32[3]{0:T(128)} %pad_add_fusion.where_ref, bf16[128,2176]{1,0:T(8,128)(2,1)} %get-tuple-element.25.refs_0_, bf16[128,2176]{1,0:T(8,128)(2,1)} %copy-done.1, bf16[2048,768]{1,0:T(8,128)(2,1)} %refs_2_.1, f32[256,128]{1,0:T(8,128)} %get-tuple-element.67.cos_ref.refs_3_, ...), custom_call_target="tpu_custom_call" | custom-call | flops 1073741824 | bytes 1073741 | tf_op jit(solution)/shard_map/query/pallas_call | solution.py:666
  87.3 12.7 %attention.2 = (f32[4,1,256]{2,1,0:T(1,128)}, f32[4,1,256]{2,1,0:T(1,128)}, f32[4,128,256]{2,1,0:T(8,128)}) custom-call(s32[3]{0:T(128)} %pad_add_fusion.where_ref, bf16[256,512]{1,0:T(8,128)(2,1)} %get-tuple-element.26.plain_ref, bf16[256,256]{1,0:T(8,128)(2,1)} %get-tuple-element.27.turned_ref, bf16[256,512]{1,0:T(8,128)(2,1)} %ku_ref.3, ...), custom_call_target="tpu_custom_call" | custom-call | flops 3221225472 | bytes 3221225 | tf_op jit(solution)/shard_map/attention/pallas_call | solution.py:684
  100.1 5.3 %collective-permute-start.32 = (bf16[512,256]{1,0:T(8,128)(2,1)S(1)}, bf16[512,256]{1,0:T(8,128)(2,1)S(1)}, u32[]{:S(2)}, u32[]{:S(2)}) collective-permute-start(bf16[512,256]{1,0:T(8,128)(2,1)S(1)} %pad_maximum_fusion.2.refs_10_), channel_id=1, source_target_pairs={{0,8},{8,0},{16,24},{24,16},{1,9},{9,1},{17,25},{25,17},{2,10},{10... | collective-permute-start | bytes 786440 | tf_op jit(solution)/shard_map/ppermute | solution.py:72
  105.4 1.6 %collective-permute-start.34 = (bf16[512,256]{1,0:T(8,128)(2,1)S(1)}, bf16[512,256]{1,0:T(8,128)(2,1)S(1)}, u32[]{:S(2)}, u32[]{:S(2)}) collective-permute-start(bf16[512,256]{1,0:T(8,128)(2,1)S(1)} %pad_maximum_fusion.2.refs_10_), channel_id=1, source_target_pairs={{0,24},{8,16},{16,8},{24,0},{1,25},{9,17},{17,9},{25,1},{2,26},{10... | collective-permute-start | bytes 786440 | tf_op jit(solution)/shard_map/ppermute | solution.py:72
  107.1 0.8 copy-done.7
  107.9 13.0 %state_scan.1 = (f32[1024,256]{1,0:T(8,128)}, bf16[1024,128]{1,0:T(8,128)(2,1)}, f32[1024,128]{1,0:T(8,128)}, bf16[144,256]{1,0:T(8,128)(2,1)}) custom-call(s32[3]{0:T(128)} %pad_add_fusion.where_ref, bf16[128,2176]{1,0:T(8,128)(2,1)} %get-tuple-element.25.refs_0_, bf16[128,2176]{1,0:T(8,128)(2,1)} %copy-done.1, bf16[128,2176]{1,0:T(8,128)(2,1)} %copy-done.2, ...), custom_call_target="tpu_custom_call" | custom-call | flops 4294967296 | bytes 4294967 | tf_op jit(solution)/shard_map/state_scan/pallas_call | solution.py:714
  120.9 2.9 %collective-permute-start.29 = (bf16[144,256]{1,0:T(8,128)(2,1)}, bf16[144,256]{1,0:T(8,128)(2,1)S(1)}, u32[]{:S(2)}, u32[]{:S(2)}) collective-permute-start(bf16[144,256]{1,0:T(8,128)(2,1)} %get-tuple-element.39), channel_id=1, source_target_pairs={{0,8},{8,0},{16,24},{24,16},{1,9},{9,1},{17,25},{25,17},{2,10},{10... | collective-permute-start | bytes 221192 | tf_op jit(solution)/shard_map/ppermute | solution.py:72
  123.8 1.5 collective-permute-start.31
  125.3 8.8 %collective-permute-done.34.refs_13_ = bf16[512,256]{1,0:T(8,128)(2,1)S(1)} collective-permute-done((bf16[512,256]{1,0:T(8,128)(2,1)S(1)}, bf16[512,256]{1,0:T(8,128)(2,1)S(1)}, u32[]{:S(2)}, u32[]{:S(2)}) %collective-permute-start.34) | collective-permute-done | bytes 262176 | tf_op jit(solution)/shard_map/ppermute | solution.py:72
  134.2 0.7 copy-done.21
  134.9 5.5 %gate.1.gate_ref = f32[1024,256]{1,0:T(8,128)} custom-call(s32[3]{0:T(128)} %pad_add_fusion.where_ref, bf16[128,2176]{1,0:T(8,128)(2,1)} %get-tuple-element.25.refs_0_, bf16[128,2176]{1,0:T(8,128)(2,1)} %copy-done.1, bf16[128,2176]{1,0:T(8,128)(2,1)} %copy-done.2, bf16[128,2176]{1,0:T(8,128)(2,1)} %copy-done.6, bf16[128,2176]{1,0:T(8,128)(2,1)} %copy-done.3, ...), custom_call_target="tpu_custom_call" | custom-call | flops 1073741824 | bytes 1073741 | tf_op jit(solution)/shard_map/gate/pallas_call | solution.py:763
  140.4 0.8 pad_maximum_fusion.1.states_ref
  141.2 4.4 %finish.1 = bf16[1024,256]{1,0:T(8,128)(2,1)} custom-call(s32[3]{0:T(128)} %pad_add_fusion.where_ref, bf16[4,144,256]{2,1,0:T(8,128)(2,1)} %pad_maximum_fusion.1.states_ref, f32[1024,256]{1,0:T(8,128)} %get-tuple-element.40.mixed_ref, bf16[1024,128]{1,0:T(8,128)(2,1)} %get-tuple-element.41.reads_ref, f32[1024,256]{1,0:T(8,128)} %gate.1.gate_ref, ...), custom_call_target="tpu_custom_call" | custom-call | tf_op jit(solution)/shard_map/finish/pallas_call | solution.py:781
  145.6 3.7 %all-to-all-start = ((bf16[4,256,256]{2,1,0:T(8,128)(2,1)}), bf16[4,256,256]{2,1,0:T(8,128)(2,1)S(1)}, u32[]{:S(2)}, u32[]{:S(2)}) async-start(bf16[4,256,256]{2,1,0:T(8,128)(2,1)} %bitcast.46), calls=%async_computation | async-start | bytes 1048576 | tf_op jit(solution)/shard_map/all_to_all | solution.py:802
  149.3 2.4 %attention.3 = bf16[256,512]{1,0:T(8,128)(2,1)} custom-call(s32[3]{0:T(128)} %pad_add_fusion.where_ref, bf16[256,512]{1,0:T(8,128)(2,1)} %get-tuple-element.26.plain_ref, bf16[256,256]{1,0:T(8,128)(2,1)} %get-tuple-element.27.turned_ref, bf16[256,512]{1,0:T(8,128)(2,1)} %ku_ref.3, bf16[512,256]{1,0:T(8,128)(2,1)} %bitcast.49, bf16[528,384]{1,0:T(8,128)(2,1)} %copy-done.5, ...), custom_call_target="tpu_custom_call" | custom-call | flops 1073741824 | bytes 1073741 | tf_op jit(solution)/shard_map/attention/pallas_call | solution.py:684
  151.7 4.7 %all-to-all-done = bf16[4,256,256]{2,1,0:T(8,128)(2,1)S(1)} async-done(((bf16[4,256,256]{2,1,0:T(8,128)(2,1)}), bf16[4,256,256]{2,1,0:T(8,128)(2,1)S(1)}, u32[]{:S(2)}, u32[]{:S(2)}) %all-to-all-start) | async-done | bytes 524320 | tf_op jit(solution)/shard_map/all_to_all | solution.py:802
  156.4 0.9 copy.30
  (132 shorter events, 5.3 us)
Async XLA Ops:
  0.7 13.3 %copy-start.27 = (f32[256,16]{0,1:T(8,128)S(1)}, f32[256,16]{0,1:T(8,128)}, u32[]{:S(2)}) copy-start(f32[256,16]{0,1:T(8,128)} %param.37) | copy-start | bytes 49156
  0.7 13.5 %copy-start.18 = (bf16[128,1024]{1,0:T(8,128)(2,1)S(1)}, bf16[128,1024]{1,0:T(8,128)(2,1)}, u32[]{:S(2)}) copy-start(bf16[128,1024]{1,0:T(8,128)(2,1)} %param.29) | copy-start | bytes 786436
  6.5 38.6 %copy-start = (bf16[128,2176]{1,0:T(8,128)(2,1)S(1)}, bf16[128,2176]{1,0:T(8,128)(2,1)}, u32[]{:S(2)}) copy-start(bf16[128,2176]{1,0:T(8,128)(2,1)} %get-tuple-element.25.refs_0_) | copy-start | bytes 1671172
  6.5 7.9 %collective-permute-start.4 = (bf16[128,384]{1,0:T(8,128)(2,1)}, bf16[128,384]{1,0:T(8,128)(2,1)S(1)}, u32[]{:S(2)}, u32[]{:S(2)}) collective-permute-start(bf16[128,384]{1,0:T(8,128)(2,1)} %get-tuple-element.30), channel_id=1, source_target_pairs={{0,8},{8,0},{16,24},{24,16},{1,9},{9,1},{17,25},{25,17},{2,10},{10... | collective-permute-start | bytes 294920 | tf_op jit(solution)/shard_map/ppermute | solution.py:72
  8.1 7.8 %collective-permute-start.5 = (bf16[128,384]{1,0:T(8,128)(2,1)}, bf16[128,384]{1,0:T(8,128)(2,1)S(1)}, u32[]{:S(2)}, u32[]{:S(2)}) collective-permute-start(bf16[128,384]{1,0:T(8,128)(2,1)} %get-tuple-element.30), channel_id=1, source_target_pairs={{0,16},{8,24},{16,0},{24,8},{1,17},{9,25},{17,1},{25,9},{2,18},{10... | collective-permute-start | bytes 294920 | tf_op jit(solution)/shard_map/ppermute | solution.py:72
  8.4 10.3 %collective-permute-start.6 = (bf16[128,384]{1,0:T(8,128)(2,1)}, bf16[128,384]{1,0:T(8,128)(2,1)S(1)}, u32[]{:S(2)}, u32[]{:S(2)}) collective-permute-start(bf16[128,384]{1,0:T(8,128)(2,1)} %get-tuple-element.30), channel_id=1, source_target_pairs={{0,24},{8,16},{16,8},{24,0},{1,25},{9,17},{17,9},{25,1},{2,26},{10... | collective-permute-start | bytes 294920 | tf_op jit(solution)/shard_map/ppermute | solution.py:72
  11.1 15.8 %collective-permute-start.1 = (bf16[128,512]{1,0:T(8,128)(2,1)S(1)}, bf16[128,512]{1,0:T(8,128)(2,1)S(1)}, u32[]{:S(2)}, u32[]{:S(2)}) collective-permute-start(bf16[128,512]{1,0:T(8,128)(2,1)S(1)} %pad_maximum_fusion.3), channel_id=1, source_target_pairs={{0,2},{2,0},{4,6},{6,4},{1,3},{3,1},{5,7},{7,5},{8,10},{10,8},{12,... | collective-permute-start | bytes 393224 | tf_op jit(solution)/shard_map/ppermute | solution.py:72
  12.6 38.7 %collective-permute-start.15 = (bf16[128,2176]{1,0:T(8,128)(2,1)}, bf16[128,2176]{1,0:T(8,128)(2,1)S(1)}, u32[]{:S(2)}, u32[]{:S(2)}) collective-permute-start(bf16[128,2176]{1,0:T(8,128)(2,1)} %get-tuple-element.25.refs_0_), channel_id=1, source_target_pairs={{0,2},{2,0},{4,6},{6,4},{1,3},{3,1},{5,7},{7,5},{8,10},{10,8},{12,... | collective-permute-start | bytes 1671176 | tf_op jit(solution)/shard_map/ppermute | solution.py:72
  14.3 12.5 %collective-permute-start.2 = (bf16[128,512]{1,0:T(8,128)(2,1)S(1)}, bf16[128,512]{1,0:T(8,128)(2,1)S(1)}, u32[]{:S(2)}, u32[]{:S(2)}) collective-permute-start(bf16[128,512]{1,0:T(8,128)(2,1)S(1)} %pad_maximum_fusion.4), channel_id=1, source_target_pairs={{0,4},{2,6},{4,0},{6,2},{1,5},{3,7},{5,1},{7,3},{8,12},{10,14},{12... | collective-permute-start | bytes 393224 | tf_op jit(solution)/shard_map/ppermute | solution.py:72
  15.9 16.4 %collective-permute-start.3 = (bf16[128,512]{1,0:T(8,128)(2,1)S(1)}, bf16[128,512]{1,0:T(8,128)(2,1)S(1)}, u32[]{:S(2)}, u32[]{:S(2)}) collective-permute-start(bf16[128,512]{1,0:T(8,128)(2,1)S(1)} %pad_maximum_fusion.5), channel_id=1, source_target_pairs={{0,6},{2,4},{4,2},{6,0},{1,7},{3,5},{5,3},{7,1},{8,14},{10,12},{12... | collective-permute-start | bytes 393224 | tf_op jit(solution)/shard_map/ppermute | solution.py:72
  18.8 6.2 %collective-permute-start.7 = (bf16[3,2048]{1,0:T(4,128)(2,1)S(1)}, bf16[3,2048]{1,0:T(4,128)(2,1)S(1)}, u32[]{:S(2)}, u32[]{:S(2)}) collective-permute-start(bf16[3,2048]{1,0:T(4,128)(2,1)S(1)} %slice.33), channel_id=1, source_target_pairs={{0,8},{8,16},{16,24},{1,9},{9,17},{17,25},{2,10},{10,18},{18,26},{... | collective-permute-start | bytes 36872 | tf_op jit(solution)/shard_map/ppermute | solution.py:627
  25.0 11.0 %collective-permute-start.28 = (bf16[144,256]{1,0:T(8,128)(2,1)S(1)}, bf16[144,256]{1,0:T(8,128)(2,1)}, u32[]{:S(2)}, u32[]{:S(2)}) collective-permute-start(bf16[144,256]{1,0:T(8,128)(2,1)S(1)} %get-tuple-element.49), channel_id=1, source_target_pairs={{0,6},{2,4},{4,2},{6,0},{1,7},{3,5},{5,3},{7,1},{8,14},{10,12},{12... | collective-permute-start | bytes 221192 | tf_op jit(solution)/shard_map/ppermute | solution.py:72
  26.9 59.9 %copy-start.5 = (bf16[528,384]{1,0:T(8,128)(2,1)}, bf16[528,384]{1,0:T(8,128)(2,1)S(1)}, u32[]{:S(2)}) copy-start(bf16[528,384]{1,0:T(8,128)(2,1)S(1)} %constant_dynamic-update-slice_fusion.refs_0_.refs_14_) | copy-start | bytes 1216516
  32.4 39.7 %copy-start.8 = (bf16[512,512]{1,0:T(8,128)(2,1)}, bf16[512,512]{1,0:T(8,128)(2,1)S(1)}, u32[]{:S(2)}) copy-start(bf16[512,512]{1,0:T(8,128)(2,1)S(1)} %pad_maximum_fusion.refs_10_) | copy-start | bytes 1572868
  32.4 17.0 %collective-permute-start.9 = (bf16[528,384]{1,0:T(8,128)(2,1)S(1)}, bf16[528,384]{1,0:T(8,128)(2,1)S(1)}, u32[]{:S(2)}, u32[]{:S(2)}) collective-permute-start(bf16[528,384]{1,0:T(8,128)(2,1)S(1)} %constant_dynamic-update-slice_fusion.refs_0_.refs_14_), channel_id=1, source_target_pairs={{0,2},{2,0},{4,6},{6,4},{1,3},{3,1},{5,7},{7,5},{8,10},{10,8},{12,... | collective-permute-start | bytes 1216520 | tf_op jit(solution)/shard_map/ppermute | solution.py:72
  33.9 17.4 %collective-permute-start.11 = (bf16[528,384]{1,0:T(8,128)(2,1)S(1)}, bf16[528,384]{1,0:T(8,128)(2,1)}, u32[]{:S(2)}, u32[]{:S(2)}) collective-permute-start(bf16[528,384]{1,0:T(8,128)(2,1)S(1)} %constant_dynamic-update-slice_fusion.refs_0_.refs_14_), channel_id=1, source_target_pairs={{0,4},{2,6},{4,0},{6,2},{1,5},{3,7},{5,1},{7,3},{8,12},{10,14},{12... | collective-permute-start | bytes 1216520 | tf_op jit(solution)/shard_map/ppermute | solution.py:72
  34.2 10.9 %collective-permute-start.27 = (bf16[144,256]{1,0:T(8,128)(2,1)S(1)}, bf16[144,256]{1,0:T(8,128)(2,1)}, u32[]{:S(2)}, u32[]{:S(2)}) collective-permute-start(bf16[144,256]{1,0:T(8,128)(2,1)S(1)} %get-tuple-element.50), channel_id=1, source_target_pairs={{0,4},{2,6},{4,0},{6,2},{1,5},{3,7},{5,1},{7,3},{8,12},{10,14},{12... | collective-permute-start | bytes 221192 | tf_op jit(solution)/shard_map/ppermute | solution.py:72
  36.0 9.1 %collective-permute-start.26 = (bf16[144,256]{1,0:T(8,128)(2,1)S(1)}, bf16[144,256]{1,0:T(8,128)(2,1)S(1)}, u32[]{:S(2)}, u32[]{:S(2)}) collective-permute-start(bf16[144,256]{1,0:T(8,128)(2,1)S(1)} %get-tuple-element.48), channel_id=1, source_target_pairs={{0,2},{2,0},{4,6},{6,4},{1,3},{3,1},{5,7},{7,5},{8,10},{10,8},{12,... | collective-permute-start | bytes 221192 | tf_op jit(solution)/shard_map/ppermute | solution.py:72
  45.1 20.4 %collective-permute-start.17 = (bf16[128,2176]{1,0:T(8,128)(2,1)S(1)}, bf16[128,2176]{1,0:T(8,128)(2,1)S(1)}, u32[]{:S(2)}, u32[]{:S(2)}) collective-permute-start(bf16[128,2176]{1,0:T(8,128)(2,1)S(1)} %copy-done), channel_id=1, source_target_pairs={{0,4},{2,6},{4,0},{6,2},{1,5},{3,7},{5,1},{7,3},{8,12},{10,14},{12... | collective-permute-start | bytes 1671176 | tf_op jit(solution)/shard_map/ppermute | solution.py:72
  45.1 31.7 %copy-start.26 = (bf16[144,256]{1,0:T(8,128)(2,1)}, bf16[144,256]{1,0:T(8,128)(2,1)S(1)}, u32[]{:S(2)}) copy-start(bf16[144,256]{1,0:T(8,128)(2,1)S(1)} %collective-permute-done.26) | copy-start | bytes 221188
  45.1 20.4 %collective-permute-start.23 = (bf16[512,512]{1,0:T(8,128)(2,1)S(1)}, bf16[512,512]{1,0:T(8,128)(2,1)}, u32[]{:S(2)}, u32[]{:S(2)}) collective-permute-start(bf16[512,512]{1,0:T(8,128)(2,1)S(1)} %pad_maximum_fusion.refs_10_), channel_id=1, source_target_pairs={{0,8},{8,16},{16,24},{24,0},{1,9},{9,17},{17,25},{25,1},{2,10},{10... | collective-permute-start | bytes 1572872 | tf_op jit(solution)/shard_map/ppermute | solution.py:81
  49.4 27.4 %copy-start.9 = (bf16[528,384]{1,0:T(8,128)(2,1)}, bf16[528,384]{1,0:T(8,128)(2,1)S(1)}, u32[]{:S(2)}) copy-start(bf16[528,384]{1,0:T(8,128)(2,1)S(1)} %collective-permute-done.9.refs_2_.refs_16_) | copy-start | bytes 1216516
  49.4 18.2 %collective-permute-start.13 = (bf16[528,384]{1,0:T(8,128)(2,1)S(1)}, bf16[528,384]{1,0:T(8,128)(2,1)}, u32[]{:S(2)}, u32[]{:S(2)}) collective-permute-start(bf16[528,384]{1,0:T(8,128)(2,1)S(1)} %constant_dynamic-update-slice_fusion.refs_0_.refs_14_), channel_id=1, source_target_pairs={{0,6},{2,4},{4,2},{6,0},{1,7},{3,5},{5,3},{7,1},{8,14},{10,12},{12... | collective-permute-start | bytes 1216520 | tf_op jit(solution)/shard_map/ppermute | solution.py:72
  51.4 16.4 %collective-permute-start.8 = (bf16[528,384]{1,0:T(8,128)(2,1)S(1)}, bf16[528,384]{1,0:T(8,128)(2,1)S(1)}, u32[]{:S(2)}, u32[]{:S(2)}) collective-permute-start(bf16[528,384]{1,0:T(8,128)(2,1)S(1)} %constant_dynamic-update-slice_fusion.refs_0_.refs_14_), channel_id=1, source_target_pairs={{0,1},{1,0},{2,3},{3,2},{4,5},{5,4},{6,7},{7,6},{8,9},{9,8},{10,11... | collective-permute-start | bytes 1216520 | tf_op jit(solution)/shard_map/ppermute | solution.py:72
  51.4 35.4 %copy-start.2 = (bf16[128,2176]{1,0:T(8,128)(2,1)}, bf16[128,2176]{1,0:T(8,128)(2,1)S(1)}, u32[]{:S(2)}) copy-start(bf16[128,2176]{1,0:T(8,128)(2,1)S(1)} %collective-permute-done.15.refs_2_) | copy-start | bytes 1671172
  51.4 18.4 %collective-permute-start = (bf16[128,2176]{1,0:T(8,128)(2,1)S(1)}, bf16[128,2176]{1,0:T(8,128)(2,1)S(1)}, u32[]{:S(2)}, u32[]{:S(2)}) collective-permute-start(bf16[128,2176]{1,0:T(8,128)(2,1)S(1)} %copy-done), channel_id=1, source_target_pairs={{0,1},{1,0},{2,3},{3,2},{4,5},{5,4},{6,7},{7,6},{8,9},{9,8},{10,11... | collective-permute-start | bytes 1671176 | tf_op jit(solution)/shard_map/ppermute | solution.py:72
  65.5 34.5 %copy-start.3 = (bf16[128,2176]{1,0:T(8,128)(2,1)}, bf16[128,2176]{1,0:T(8,128)(2,1)S(1)}, u32[]{:S(2)}) copy-start(bf16[128,2176]{1,0:T(8,128)(2,1)S(1)} %collective-permute-done.17.refs_4_) | copy-start | bytes 1671172
  65.5 6.5 %collective-permute-start.19 = (bf16[64,2176]{1,0:T(8,128)(2,1)S(1)}, bf16[64,2176]{1,0:T(8,128)(2,1)S(1)}, u32[]{:S(2)}, u32[]{:S(2)}) collective-permute-start(bf16[64,2176]{1,0:T(8,128)(2,1)S(1)} %slice.44), channel_id=1, source_target_pairs={{0,4},{2,6},{4,0},{6,2},{1,5},{3,7},{5,1},{7,3},{8,12},{10,14},{12... | collective-permute-start | bytes 835592 | tf_op jit(solution)/shard_map/ppermute | solution.py:72
  65.5 11.9 %collective-permute-start.24 = (bf16[512,512]{1,0:T(8,128)(2,1)}, bf16[512,512]{1,0:T(8,128)(2,1)}, u32[]{:S(2)}, u32[]{:S(2)}) collective-permute-start(bf16[512,512]{1,0:T(8,128)(2,1)} %collective-permute-done.23.refs_11_), channel_id=1, source_target_pairs={{0,8},{8,16},{16,24},{24,0},{1,9},{9,17},{17,25},{25,1},{2,10},{10... | collective-permute-start | bytes 1572872 | tf_op jit(solution)/shard_map/ppermute | solution.py:81
  67.6 9.2 %collective-permute-start.10 = (bf16[528,384]{1,0:T(8,128)(2,1)S(1)}, bf16[528,384]{1,0:T(8,128)(2,1)S(1)}, u32[]{:S(2)}, u32[]{:S(2)}) collective-permute-start(bf16[528,384]{1,0:T(8,128)(2,1)S(1)} %collective-permute-done.9.refs_2_.refs_16_), channel_id=1, source_target_pairs={{0,1},{1,0},{2,3},{3,2},{4,5},{5,4},{6,7},{7,6},{8,9},{9,8},{10,11... | collective-permute-start | bytes 1216520 | tf_op jit(solution)/shard_map/ppermute | solution.py:72
  67.7 13.8 %copy-start.10 = (bf16[528,384]{1,0:T(8,128)(2,1)}, bf16[528,384]{1,0:T(8,128)(2,1)S(1)}, u32[]{:S(2)}) copy-start(bf16[528,384]{1,0:T(8,128)(2,1)S(1)} %collective-permute-done.8.refs_1_.refs_15_) | copy-start | bytes 1216516
  67.7 9.0 %collective-permute-start.21 = (bf16[64,2176]{1,0:T(8,128)(2,1)S(1)}, bf16[64,2176]{1,0:T(8,128)(2,1)S(1)}, u32[]{:S(2)}, u32[]{:S(2)}) collective-permute-start(bf16[64,2176]{1,0:T(8,128)(2,1)S(1)} %slice.45), channel_id=1, source_target_pairs={{0,2},{2,0},{4,6},{6,4},{1,3},{3,1},{5,7},{7,5},{8,10},{10,8},{12,... | collective-permute-start | bytes 835592 | tf_op jit(solution)/shard_map/ppermute | solution.py:72
  69.8 16.9 %collective-permute-start.12 = (bf16[528,384]{1,0:T(8,128)(2,1)}, bf16[528,384]{1,0:T(8,128)(2,1)}, u32[]{:S(2)}, u32[]{:S(2)}) collective-permute-start(bf16[528,384]{1,0:T(8,128)(2,1)} %collective-permute-done.11.refs_4_.refs_18_), channel_id=1, source_target_pairs={{0,1},{1,0},{2,3},{3,2},{4,5},{5,4},{6,7},{7,6},{8,9},{9,8},{10,11... | collective-permute-start | bytes 1216520 | tf_op jit(solution)/shard_map/ppermute | solution.py:72
  72.0 14.8 %collective-permute-start.14 = (bf16[528,384]{1,0:T(8,128)(2,1)}, bf16[528,384]{1,0:T(8,128)(2,1)}, u32[]{:S(2)}, u32[]{:S(2)}) collective-permute-start(bf16[528,384]{1,0:T(8,128)(2,1)} %collective-permute-done.13.refs_6_.refs_20_), channel_id=1, source_target_pairs={{0,1},{1,0},{2,3},{3,2},{4,5},{5,4},{6,7},{7,6},{8,9},{9,8},{10,11... | collective-permute-start | bytes 1216520 | tf_op jit(solution)/shard_map/ppermute | solution.py:72
  76.8 28.6 %collective-permute-start.16 = (bf16[128,2176]{1,0:T(8,128)(2,1)S(1)}, bf16[128,2176]{1,0:T(8,128)(2,1)S(1)}, u32[]{:S(2)}, u32[]{:S(2)}) collective-permute-start(bf16[128,2176]{1,0:T(8,128)(2,1)S(1)} %collective-permute-done.15.refs_2_), channel_id=1, source_target_pairs={{0,1},{1,0},{2,3},{3,2},{4,5},{5,4},{6,7},{7,6},{8,9},{9,8},{10,11... | collective-permute-start | bytes 1671176 | tf_op jit(solution)/shard_map/ppermute | solution.py:72
  76.8 30.2 %collective-permute-start.18 = (bf16[128,2176]{1,0:T(8,128)(2,1)S(1)}, bf16[128,2176]{1,0:T(8,128)(2,1)S(1)}, u32[]{:S(2)}, u32[]{:S(2)}) collective-permute-start(bf16[128,2176]{1,0:T(8,128)(2,1)S(1)} %collective-permute-done.17.refs_4_), channel_id=1, source_target_pairs={{0,1},{1,0},{2,3},{3,2},{4,5},{5,4},{6,7},{7,6},{8,9},{9,8},{10,11... | collective-permute-start | bytes 1671176 | tf_op jit(solution)/shard_map/ppermute | solution.py:72
  77.4 29.7 %collective-permute-start.25 = (bf16[512,512]{1,0:T(8,128)(2,1)}, bf16[512,512]{1,0:T(8,128)(2,1)}, u32[]{:S(2)}, u32[]{:S(2)}) collective-permute-start(bf16[512,512]{1,0:T(8,128)(2,1)} %collective-permute-done.24.refs_12_), channel_id=1, source_target_pairs={{0,8},{8,16},{16,24},{24,0},{1,9},{9,17},{17,25},{25,1},{2,10},{10... | collective-permute-start | bytes 1572872 | tf_op jit(solution)/shard_map/ppermute | solution.py:81
  82.4 23.0 %copy-start.4 = (bf16[512,256]{1,0:T(8,128)(2,1)}, bf16[512,256]{1,0:T(8,128)(2,1)S(1)}, u32[]{:S(2)}) copy-start(bf16[512,256]{1,0:T(8,128)(2,1)S(1)} %pad_maximum_fusion.2.refs_10_) | copy-start | bytes 786436
  86.8 13.3 %collective-permute-start.20 = (bf16[64,2176]{1,0:T(8,128)(2,1)S(1)}, bf16[64,2176]{1,0:T(8,128)(2,1)S(1)}, u32[]{:S(2)}, u32[]{:S(2)}) collective-permute-start(bf16[64,2176]{1,0:T(8,128)(2,1)S(1)} %copy-done.13), channel_id=1, source_target_pairs={{0,1},{1,0},{2,3},{3,2},{4,5},{5,4},{6,7},{7,6},{8,9},{9,8},{10,11... | collective-permute-start | bytes 835592 | tf_op jit(solution)/shard_map/ppermute | solution.py:72
  86.9 18.5 %collective-permute-start.22 = (bf16[64,2176]{1,0:T(8,128)(2,1)S(1)}, bf16[64,2176]{1,0:T(8,128)(2,1)S(1)}, u32[]{:S(2)}, u32[]{:S(2)}) collective-permute-start(bf16[64,2176]{1,0:T(8,128)(2,1)S(1)} %copy-done.15), channel_id=1, source_target_pairs={{0,1},{1,0},{2,3},{3,2},{4,5},{5,4},{6,7},{7,6},{8,9},{9,8},{10,11... | collective-permute-start | bytes 835592 | tf_op jit(solution)/shard_map/ppermute | solution.py:72
  100.1 23.7 %collective-permute-start.32 = (bf16[512,256]{1,0:T(8,128)(2,1)S(1)}, bf16[512,256]{1,0:T(8,128)(2,1)S(1)}, u32[]{:S(2)}, u32[]{:S(2)}) collective-permute-start(bf16[512,256]{1,0:T(8,128)(2,1)S(1)} %pad_maximum_fusion.2.refs_10_), channel_id=1, source_target_pairs={{0,8},{8,0},{16,24},{24,16},{1,9},{9,1},{17,25},{25,17},{2,10},{10... | collective-permute-start | bytes 786440 | tf_op jit(solution)/shard_map/ppermute | solution.py:72
  105.4 19.9 %collective-permute-start.33 = (bf16[512,256]{1,0:T(8,128)(2,1)S(1)}, bf16[512,256]{1,0:T(8,128)(2,1)S(1)}, u32[]{:S(2)}, u32[]{:S(2)}) collective-permute-start(bf16[512,256]{1,0:T(8,128)(2,1)S(1)} %pad_maximum_fusion.2.refs_10_), channel_id=1, source_target_pairs={{0,16},{8,24},{16,0},{24,8},{1,17},{9,25},{17,1},{25,9},{2,18},{10... | collective-permute-start | bytes 786440 | tf_op jit(solution)/shard_map/ppermute | solution.py:72
  105.4 28.7 %collective-permute-start.34 = (bf16[512,256]{1,0:T(8,128)(2,1)S(1)}, bf16[512,256]{1,0:T(8,128)(2,1)S(1)}, u32[]{:S(2)}, u32[]{:S(2)}) collective-permute-start(bf16[512,256]{1,0:T(8,128)(2,1)S(1)} %pad_maximum_fusion.2.refs_10_), channel_id=1, source_target_pairs={{0,24},{8,16},{16,8},{24,0},{1,25},{9,17},{17,9},{25,1},{2,26},{10... | collective-permute-start | bytes 786440 | tf_op jit(solution)/shard_map/ppermute | solution.py:72
  120.9 19.5 %collective-permute-start.29 = (bf16[144,256]{1,0:T(8,128)(2,1)}, bf16[144,256]{1,0:T(8,128)(2,1)S(1)}, u32[]{:S(2)}, u32[]{:S(2)}) collective-permute-start(bf16[144,256]{1,0:T(8,128)(2,1)} %get-tuple-element.39), channel_id=1, source_target_pairs={{0,8},{8,0},{16,24},{24,16},{1,9},{9,1},{17,25},{25,17},{2,10},{10... | collective-permute-start | bytes 221192 | tf_op jit(solution)/shard_map/ppermute | solution.py:72
  123.8 16.6 %collective-permute-start.30 = (bf16[144,256]{1,0:T(8,128)(2,1)}, bf16[144,256]{1,0:T(8,128)(2,1)S(1)}, u32[]{:S(2)}, u32[]{:S(2)}) collective-permute-start(bf16[144,256]{1,0:T(8,128)(2,1)} %get-tuple-element.39), channel_id=1, source_target_pairs={{0,16},{8,24},{16,0},{24,8},{1,17},{9,25},{17,1},{25,9},{2,18},{10... | collective-permute-start | bytes 221192 | tf_op jit(solution)/shard_map/ppermute | solution.py:72
  123.8 16.6 %copy-start.25 = (bf16[144,256]{1,0:T(8,128)(2,1)S(1)}, bf16[144,256]{1,0:T(8,128)(2,1)}, u32[]{:S(2)}) copy-start(bf16[144,256]{1,0:T(8,128)(2,1)} %get-tuple-element.39) | copy-start | bytes 221188
  123.8 16.6 %collective-permute-start.31 = (bf16[144,256]{1,0:T(8,128)(2,1)}, bf16[144,256]{1,0:T(8,128)(2,1)S(1)}, u32[]{:S(2)}, u32[]{:S(2)}) collective-permute-start(bf16[144,256]{1,0:T(8,128)(2,1)} %get-tuple-element.39), channel_id=1, source_target_pairs={{0,24},{8,16},{16,8},{24,0},{1,25},{9,17},{17,9},{25,1},{2,26},{10... | collective-permute-start | bytes 221192 | tf_op jit(solution)/shard_map/ppermute | solution.py:72
  145.6 10.8 %all-to-all-start = ((bf16[4,256,256]{2,1,0:T(8,128)(2,1)}), bf16[4,256,256]{2,1,0:T(8,128)(2,1)S(1)}, u32[]{:S(2)}, u32[]{:S(2)}) async-start(bf16[4,256,256]{2,1,0:T(8,128)(2,1)} %bitcast.46), calls=%async_computation | async-start | bytes 1048576 | tf_op jit(solution)/shard_map/all_to_all | solution.py:802
  (16 other events, 100.8 us)
where the time goes:
time: 158 us; the launch traced here: 157 us
  waiting for transfers between devices  49.8 us (32%)
  starting transfers between devices  46.4 us (29%)
  Pallas kernels  46.1 us (29%)
  local copies, waits for them, and re-layouts  10.3 us (7%)
  other arithmetic  3.38 us (2%)
    ppermute x31, waiting for transfers between devices, across(): return lax.ppermute(value, axis, [(i, i ^ k) for i in range(count)])  43.7 us
    ppermute x31, starting transfers between devices, across(): return lax.ppermute(value, axis, [(i, i ^ k) for i in range(count)])  32.1 us
    pallas_call x2, Pallas kernels, attend(): pl.pallas_call(functools.partial(attention_kernel, planes=B, cores=T, slo...  15.1 us
    pallas_call x1, Pallas kernels, shards(): pl.pallas_call(functools.partial(scan_kernel, parts=tuple(parts), planes=...  13 us
    ppermute x3, starting transfers between devices, ring(): pieces.append(lax.ppermute(pieces[-1], axis, pairs))  5.76 us
    pallas_call x1, Pallas kernels, shards(): pl.pallas_call(functools.partial(gate_kernel, parts=tuple(parts), planes=...  5.5 us
    ppermute x1, starting transfers between devices, shards(): lax.ppermute(own[rows - taps + 1:, :model], 'a', [(i, i + 1) for i in ran...  4.79 us
    all_to_all x1, waiting for transfers between devices, shards(): lax.all_to_all(scanned.reshape(B, length, channels), 'b', 0, 0, tiled=True)  4.65 us
  transfers between devices with their start and end apart: 36, of which 9 were waited for; matrix products, arithmetic and copies ran while one was open for 5% of the time, Pallas kernels for 24%

commit v1 on v0

--- a/solution.py
+++ b/solution.py
@@ -75,10 +75,14 @@
 def ring(value, axis):
     count = lax.axis_size(axis)
     if count <= DIRECT:
-        pieces = [value]
-        for _ in range(1, count):
-            pairs = [(i, (i + 1) % count) for i in range(count)]
-            pieces.append(lax.ppermute(pieces[-1], axis, pairs))
+        pieces = [value] + [None] * (count - 1)
+        for way, steps in ((1, count // 2), (-1, (count - 1) // 2)):
+            moving = value
+            for step in range(1, steps + 1):
+                place = way * step % count
+                pairs = [(i, (i + way) % count) for i in range(count)]
+                moving = lax.ppermute(moving, axis, pairs)
+                pieces[place] = moving
         return pieces
     everything = lax.all_gather(value, axis)
     here = lax.axis_index(axis)
@@ -96,13 +100,14 @@
 
 
 def prologue_kernel(
-    where_ref, tokens_ref, mix_ref, proj_ref, gain_ref, rope_ref, step_ref, cos_ref, sin_ref, rows_ref, key_ref
+    where_ref, tokens_ref, mix_ref, proj_ref, gain_ref, rope_ref, step_ref, cos_ref, sin_ref, rows_ref, key_ref, edge_ref
 ):
     tokens = tokens_ref[...].astype(f32)
     scale = lax.rsqrt(jnp.mean(tokens * tokens, axis=-1, keepdims=True) + eps)
     x = (tokens * scale * mix_ref[...]).astype(bf16)
     model = x.shape[1]
     rows_ref[:, :model] = x
+    edge_ref[...] = x[x.shape[0] - edge_ref.shape[0] :, :]
     wide = nn(x, proj_ref[...])
     scale = lax.rsqrt(jnp.mean(wide * wide, axis=-1, keepdims=True) + eps)
     width = wide.shape[1]
@@ -308,9 +313,8 @@
     nx = len(parts)
     xs_in = refs[:nx]
     ws_in = refs[nx : nx + weights]
-    halo_in = refs[nx + weights : nx + weights + planes * cores]
+    tails_in = refs[nx + weights : nx + weights + planes * cores]
     (
-        extra_ref,
         ci_ref,
         cw_ref,
         cr_ref,
@@ -318,33 +322,35 @@
         skip_ref,
         mixed_ref,
         reads_ref,
+        gate_ref,
         run_ref,
         state_ref,
         xs,
         ws,
-        hs,
         hx,
-        pad,
+        raws,
         state_s,
         base_s,
         xsem,
         wsem,
-        hsem,
+        tails,
+        tsem,
     ) = refs[nx + weights + planes * cores :]
     ia, ib, it = where_ref[0], where_ref[1], where_ref[2]
     deep = ws_in[0].shape[0]
     channels = heads * SSM_DIM
+    conv = channels + 2 * SSM_STATE
     span = ci_ref.shape[0]
-    tiles = hs.shape[0]
-    bottom = halo_in[0].shape[0] - tiles
+    bottom = tails_in[0].shape[0] - tails.shape[1]
     for k in range(planes):
         for t in range(cores):
+            piece = tails_in[k * cores + t].at[pl.ds(bottom, tails.shape[1]), :]
+            if t == 0:
+                pltpu.make_async_copy(piece, tails.at[k], tsem.at[k]).start()
 
             @pl.when(((ib ^ k) == planes - 1) & ((it ^ t) == cores - 1))
             def _():
-                pltpu.make_async_copy(
-                    halo_in[k * cores + t].at[pl.ds(bottom, tiles), :], hs, hsem
-                ).start()
+                pltpu.make_async_copy(piece, tails.at[planes], tsem.at[planes]).start()
 
     for k in range(weights):
         for copy in weight_copies(
@@ -355,15 +361,17 @@
         copy.start()
     state_s[...] = jnp.zeros(state_s.shape, f32)
     base_s[...] = jnp.zeros(base_s.shape, f32)
-    pltpu.make_async_copy(hs, hs, hsem).wait()
-    edge = hs[...].astype(f32)
+    for k in range(planes):
+        pltpu.make_async_copy(tails.at[k], tails.at[k], tsem.at[k]).wait()
+    pltpu.make_async_copy(tails.at[planes], tails.at[planes], tsem.at[planes]).wait()
+    edge = tails[planes, :, length:].astype(f32)
     hx[...] = jnp.zeros(hx.shape, f32)
-    for i in range(tiles):
-        for r in range(span - 1):
-            row = 8 - (span - 1) + r
-            hx[row : row + 1, i * LANES : (i + 1) * LANES] = edge[
-                i : i + 1, r * LANES : (r + 1) * LANES
-            ]
+    each = edge.shape[0] // (span - 1)
+    for r in range(span - 1):
+        row = 8 - (span - 1) + r
+        for i in range(each):
+            at = r * each + i
+            hx[row : row + 1, i * LANES : (i + 1) * LANES] = edge[at : at + 1, :]
     lane = lax.broadcasted_iota(jnp.int32, (length, LANES), 1)
     li = lax.broadcasted_iota(jnp.int32, (length, length), 0)
     si = lax.broadcasted_iota(jnp.int32, (length, length), 1)
@@ -386,7 +394,9 @@
         lambda i, j: (i % every == first + j % heads) & (i < 3 * every) & (j < 3 * heads),
     ).astype(bf16)
     pick_offset = onehot(
-        16, LANES, lambda i, j: (i % heads == j % heads) & (i < 3 * heads) & (j < 3 * heads)
+        tails.shape[1],
+        LANES,
+        lambda i, j: (i % local == ib * heads + j % heads) & (i < 3 * local) & (j < 3 * heads),
     ).astype(bf16)
     pick_rate = onehot(local, LANES, lambda i, j: (i == ib * heads + j % heads) & (j < 3 * heads))
     pick_skip = onehot(local, channels, lambda i, j: i == ib * heads + j // SSM_DIM)
@@ -402,24 +412,30 @@
     )
     for k in range(weights):
         pltpu.make_async_copy(ws_in[k], ws.at[pl.ds(0, deep), :], wsem.at[k]).wait()
-    pad[0:8, :] = nn(hx[...].astype(bf16), ws[...]).astype(bf16).astype(f32)
-
-    def chunk(c, carry):
-        here = pl.ds(pl.multiple_of(c * length, length), length)
+    raws[0, 0:8, :] = nn(hx[...].astype(bf16), ws[:, :conv]).astype(bf16).astype(f32)
+
+    def product(c):
+        here = pl.ds(c * length, length)
         pltpu.make_async_copy(xs.at[here, :], xs.at[here, :], xsem.at[c]).wait()
         raw = nn(xs[here, :model], ws[...]).astype(bf16)
-        pad[8:, :] = raw.astype(f32)
-        total = jnp.zeros(raw.shape, f32)
+        gate_ref[here, :] = raw[:, conv:]
+        raw = raw[:, :conv].astype(f32)
+        raws[c, 8:, :] = raw
+        if c + 1 < planes:
+            raws[c + 1, 0:8, :] = raw[length - 8 :, :]
+
+    def chunk(c):
+        here = pl.ds(c * length, length)
+        total = jnp.zeros((length, raws.shape[2]), f32)
         for k in range(span):
-            total = total + taps[k : k + 1, :] * pad[8 - span + 1 + k : 8 - span + 1 + k + length, :]
+            total = total + taps[k : k + 1, :] * raws[c, pl.ds(8 - span + 1 + k, length), :]
         mixed_in = jax.nn.silu(total).astype(bf16)
-        pad[0:8, :] = pad[length : length + 8, :]
         head = mixed_in[:, :channels].astype(f32)
         write = mixed_in[:, channels : channels + SSM_STATE]
         read = mixed_in[:, channels + SSM_STATE :]
         reads_ref[here, :] = read
         step = nn(xs[here, model:], pick)
-        offset = tn(extra_ref[ib ^ c], pick_offset)
+        offset = tn(tails[ib ^ c][:, :length], pick_offset)
         decay = rate * step + offset
         high = decay.astype(bf16)
         rest = decay - high.astype(f32)
@@ -452,9 +468,10 @@
         to_end = jnp.exp(wide_heads(ending - running, heads, lane))
         update = tn(write, (stepped * to_end).astype(bf16))
         state_s[...] = state_s[...] * reach[length - 1 :, :] + update
-        return carry
-
-    lax.fori_loop(0, planes, chunk, 0)
+
+    for c in range(planes):
+        product(c)
+        chunk(c)
     state_ref[: SSM_STATE, :] = state_s[...].astype(bf16)
     total = wide_heads(base_s[...], heads, lane[:1])
     high = total.astype(bf16)
@@ -467,36 +484,6 @@
     state_ref[SSM_STATE :, :] = tail
 
 
-def gate_kernel(where_ref, *refs, parts, planes, cores, weights, length):
-    nx = len(parts)
-    xs_in = refs[:nx]
-    ws_in = refs[nx : nx + weights]
-    out_ref, xs, ws, xsem, wsem = refs[nx + weights :]
-    ia = where_ref[0]
-    deep = ws_in[0].shape[0]
-    model = ws.shape[0]
-
-    for k in range(weights):
-        for copy in weight_copies(where_ref, ws_in[k], ia ^ k, ws, wsem.at[k], planes):
-            copy.start()
-    for copy in row_copies(where_ref, xs_in, parts, xs, xsem, length, cores, model):
-        copy.start()
-    for k in range(weights):
-        pltpu.make_async_copy(ws_in[k], ws.at[pl.ds(0, deep), :], wsem.at[k]).wait()
-    batch = 2 if planes % 2 == 0 else 1
-
-    def some(c, carry):
-        for i in range(batch):
-            block = c * batch + i
-            at = pl.ds(pl.multiple_of(block * length, length), length)
-            pltpu.make_async_copy(xs.at[at, :], xs.at[at, :], xsem.at[block]).wait()
-        here = pl.ds(pl.multiple_of(c * batch * length, batch * length), batch * length)
-        out_ref[here, :] = jax.nn.silu(nn(xs[here, :], ws[...]).astype(bf16).astype(f32))
-        return carry
-
-    lax.fori_loop(0, planes // batch, some, 0)
-
-
 def finish_kernel(
     where_ref, states_ref, mixed_ref, reads_ref, gate_ref, run_ref, gain_ref, out_ref, into_s, *, heads
 ):
@@ -523,7 +510,7 @@
     lane = lax.broadcasted_iota(jnp.int32, (rows, LANES), 1)
     reach = jnp.exp(wide_heads(run_ref[...], heads, lane))
     mixed = mixed_ref[...] + nn(reads_ref[...], into_s[...].astype(bf16)) * reach
-    gated = mixed * gate_ref[...]
+    gated = mixed * jax.nn.silu(gate_ref[...].astype(f32))
     scale = lax.rsqrt(jnp.mean(gated * gated, axis=-1, keepdims=True) + eps)
     gain = gain_ref[:, pl.ds(pl.multiple_of(where_ref[1] * channels, channels), channels)]
     out_ref[...] = (gated * scale * gain).astype(bf16)
@@ -574,13 +561,12 @@
     local = decay_log.shape[0]
     per_group = local // groups
     channels = per_group * SSM_DIM
-    depth = scan_write.shape[0]
     every = step_proj.shape[1]
     taps = conv_input.shape[0]
     span = B * length
     assert groups == B and channels == length
     assert 3 * every <= LANES and 3 * per_group <= 16
-    assert (taps - 1) * LANES == key_width
+    assert length + LANES == key_width and 3 * local <= (taps - 1) * model // LANES
 
     def regrouped(pieces):
         moved = []
@@ -602,10 +588,14 @@
     cosine = jnp.cos(angle)
     sine = jnp.sin(angle) * sign[None, :]
 
-    own, key_own = pl.pallas_call(
+    own, key_own, edge = pl.pallas_call(
         prologue_kernel,
         in_specs=[smem()] + [vmem()] * 8,
-        out_shape=(shape((rows, model + LANES), bf16), shape((rows, key_width), bf16)),
+        out_shape=(
+            shape((rows, model + LANES), bf16),
+            shape((rows, key_width), bf16),
+            shape((8, model), bf16),
+        ),
         compiler_params=params(),
         cost_estimate=cost(2 * rows * model * 1024),
         name="prologue",
@@ -621,28 +611,36 @@
         sine,
     )
     scan_input, key_own = lax.optimization_barrier((scan_input, key_own))
-    packed = regrouped([(scan_input, channels), (scan_write, SSM_STATE), (scan_read, SSM_STATE)])
+    packed = regrouped(
+        [
+            (scan_input, channels),
+            (scan_write, SSM_STATE),
+            (scan_read, SSM_STATE),
+            (scan_gate, channels),
+        ],
+    )
     packed = jnp.concatenate(packed, axis=0)
 
-    edge = lax.ppermute(
-        own[rows - taps + 1 :, :model], "a", [(i, i + 1) for i in range(A - 1)]
-    )
-    edge = edge.reshape(taps - 1, model // LANES, LANES)
-    edge = jnp.transpose(edge, (1, 0, 2)).reshape(model // LANES, key_width)
-    key_stack = jnp.concatenate(exchange(key_own, "a") + [edge], axis=0)
+    edge = lax.ppermute(edge, "a", [(i, i + 1) for i in range(A - 1)])
+    edge = edge[8 - taps + 1 :].reshape(-1, LANES)
+    offsets = three_parts(decay_offset.T).reshape(3 * local, length)
+    offsets = jnp.pad(offsets, ((0, edge.shape[0] - 3 * local), (0, 0)))
+    tail = jnp.concatenate([offsets, edge], axis=1)
+    key_stack = jnp.concatenate(exchange(key_own, "a") + [tail], axis=0)
     packed, key_stack = lax.optimization_barrier((packed, key_stack))
     w_pieces = ring(packed, "a")
     key_pieces = []
-    for piece in exchange(key_stack, "b"):
+    if B == 4:
+        kside, kfront = across(key_stack, "b", 1), across(key_stack, "b", 2)
+        cut = key_stack.shape[0] // 2
+        kfar = jnp.concatenate([across(kside[:cut], "b", 2), across(kfront[cut:], "b", 1)], axis=0)
+        key_planes = [key_stack, kside, kfront, kfar]
+    else:
+        key_planes = exchange(key_stack, "b")
+    for piece in key_planes:
         key_pieces += exchange(piece, "tp")
 
-    if B == 4:
-        side, front = across(own, "b", 1), across(own, "b", 2)
-        some = rows // 2
-        far = [across(side[:some], "b", 2), across(front[some:], "b", 1)]
-        plane = [(0, 0, own), (1, 0, side), (2, 0, front), (3, 0, far[0]), (3, some, far[1])]
-    else:
-        plane = [(k, 0, piece) for k, piece in enumerate(exchange(own, "b"))]
+    plane = [(k, 0, piece) for k, piece in enumerate(exchange(own, "b"))]
     x_pieces = []
     parts = []
     for k, start, piece in plane:
@@ -650,13 +648,6 @@
             x_pieces.append(part)
             parts.append((k, t, start, part.shape[0]))
 
-    offsets = three_parts(decay_offset.T).reshape(3, groups, per_group, length)
-    offsets = jnp.transpose(offsets, (1, 0, 2, 3)).reshape(groups, 3 * per_group, length)
-    offsets = jnp.pad(offsets, ((0, 0), (0, 16 - 3 * per_group), (0, 0)))
-    offsets = jnp.transpose(offsets, (1, 0, 2)).reshape(16, groups * length)
-    extra = regrouped([(jnp.concatenate([scan_gate, offsets], axis=0), channels)])
-    g_pieces = exchange(jnp.concatenate([e[:depth] for e in extra], axis=0), "a")
-    tails = jnp.stack([e[depth:] for e in extra])
     value_t = value_up_weight.T
 
     even = heads + heads % 2
@@ -711,7 +702,7 @@
     then, carry = lax.optimization_barrier((where, carry))
 
     conv = channels + 2 * SSM_STATE
-    mixed, reads, run, state = pl.pallas_call(
+    mixed, reads, gate, run, state = pl.pallas_call(
         functools.partial(
             scan_kernel,
             parts=tuple(parts),
@@ -722,25 +713,26 @@
             heads=per_group,
             every=every,
         ),
-        in_specs=[smem()] + [hbm()] * (len(parts) + A + B * T) + [vmem()] * 6,
-        out_specs=[vmem()] * 4,
+        in_specs=[smem()] + [hbm()] * (len(parts) + A + B * T) + [vmem()] * 5,
+        out_specs=[vmem()] * 5,
         out_shape=(
             shape((span, channels), f32),
             shape((span, SSM_STATE), bf16),
+            shape((span, channels), bf16),
             shape((span, LANES), f32),
             shape((SSM_STATE + SSM_STATE // 8, channels), bf16),
         ),
         scratch_shapes=[
             pltpu.VMEM((span, model + LANES), bf16),
-            pltpu.VMEM((model, conv), bf16),
-            pltpu.VMEM((model // LANES, key_width), bf16),
+            pltpu.VMEM((model, conv + channels), bf16),
             pltpu.VMEM((8, model), f32),
-            pltpu.VMEM((8 + length, conv), f32),
+            pltpu.VMEM((B, 8 + length, conv), f32),
             pltpu.VMEM((SSM_STATE, channels), f32),
             pltpu.VMEM((1, LANES), f32),
             pltpu.SemaphoreType.DMA((B,)),
             pltpu.SemaphoreType.DMA((A,)),
-            pltpu.SemaphoreType.DMA,
+            pltpu.VMEM((B + 1,) + tail.shape, bf16),
+            pltpu.SemaphoreType.DMA((B + 1,)),
         ],
         compiler_params=params(),
         cost_estimate=cost(4 * span * model * conv),
@@ -750,7 +742,6 @@
         *x_pieces,
         *w_pieces,
         *key_pieces,
-        tails,
         conv_input,
         conv_write,
         conv_read,
@@ -760,23 +751,8 @@
 
     states = jnp.stack(exchange(state, "a"))
     then, mixed = lax.optimization_barrier((then, mixed))
-    gate = pl.pallas_call(
-        functools.partial(
-            gate_kernel, parts=tuple(parts), planes=B, cores=T, weights=A, length=length
-        ),
-        in_specs=[smem()] + [hbm()] * (len(parts) + A),
-        out_specs=vmem(),
-        out_shape=shape((span, channels), f32),
-        scratch_shapes=[
-            pltpu.VMEM((span, model), bf16),
-            pltpu.VMEM((model, channels), bf16),
-            pltpu.SemaphoreType.DMA((B,)),
-            pltpu.SemaphoreType.DMA((A,)),
-        ],
-        compiler_params=params(),
-        cost_estimate=cost(2 * span * model * channels),
-        name="gate",
-    )(then, *x_pieces, *g_pieces)
+    (attended,) = attend(then, first_part, A * B, carry)
+    gate, attended = lax.optimization_barrier((gate, attended))
 
     scanned = pl.pallas_call(
         functools.partial(finish_kernel, heads=per_group),
@@ -796,8 +772,6 @@
         compiler_params=params(),
         name="finish",
     )(where, states, mixed, reads, gate, run, group_gain.reshape(1, -1))
-    last, scanned = lax.optimization_barrier((then, scanned))
-    (attended,) = attend(last, first_part, A * B, carry)
     if B > 1:
         scanned = lax.all_to_all(scanned.reshape(B, length, channels), "b", 0, 0, tiled=True)
         scanned = jnp.transpose(scanned, (1, 0, 2)).reshape(length, B * channels)

time: 158 us -> 152 us (0.962)
  the two profiles are of different devices: /device:TPU:16 before, /device:TPU:0 now
where the time goes in v1:
time: 152 us
  waiting for transfers between devices  64.1 us (42%)
  starting transfers between devices  35.8 us (24%)
  Pallas kernels  32.2 us (21%)
  blocking collectives  12 us (8%)
  local copies, waits for them, and re-layouts  3.61 us (2%)
  other arithmetic  2.83 us (2%)
    ppermute x24, waiting for transfers between devices, across(): return lax.ppermute(value, axis, [(i, i ^ k) for i in range(count)])  39 us
    ppermute x24, starting transfers between devices, across(): return lax.ppermute(value, axis, [(i, i ^ k) for i in range(count)])  28.2 us
    ppermute x3, waiting for transfers between devices, ring(): moving = lax.ppermute(moving, axis, pairs)  23.7 us
    pallas_call x1, Pallas kernels, shards(): pl.pallas_call(functools.partial(scan_kernel, parts=tuple(parts), planes=...  13.2 us
    all_to_all x1, blocking collectives, shards(): lax.all_to_all(scanned.reshape(B, length, channels), 'b', 0, 0, tiled=True)  12 us
    pallas_call x2, Pallas kernels, attend(): pl.pallas_call(functools.partial(attention_kernel, planes=B, cores=T, slo...  6.74 us
    ppermute x3, starting transfers between devices, ring(): moving = lax.ppermute(moving, axis, pairs)  4.4 us
    pallas_call x1, Pallas kernels, shards(): pl.pallas_call(functools.partial(finish_kernel, heads=per_group), grid=(B...  4.35 us
  transfers between devices with their start and end apart: 28, of which 10 were waited for; matrix products, arithmetic and copies ran while one was open for 2% of the time, Pallas kernels for 7%

profile of v1, /device:TPU:0, one launch (start us, length us, event | category | flops | bytes accessed | tf_op | source)
XLA Modules:
  0.0 151.8 jit_solution(9491814392992705503)
XLA Ops:
  0.8 0.7 pad_add_fusion.where_ref
  1.5 1.2 fusion
  2.7 3.8 %prologue.1 = (bf16[128,2176]{1,0:T(8,128)(2,1)}, bf16[128,384]{1,0:T(8,128)(2,1)}, bf16[8,2048]{1,0:T(8,128)(2,1)}) custom-call(s32[3]{0:T(128)} %pad_add_fusion.where_ref, bf16[128,2048]{1,0:T(8,128)(2,1)} %tokens_ref.1, f32[1,2048]{1,0:T(1,128)} %bitcast.51, bf16[2048,256]{1,0:T(8,128)(2,1)} %proj_ref.1, f32[1,256]{1,0:T(1,128)} %bitcast.53, ...), custom_call_target="tpu_custom_call" | custom-call | flops 536870912 | bytes 536870 | tf_op jit(solution)/shard_map/prologue/pallas_call | solution.py:591
  6.5 5.1 %collective-permute-start.6 = (bf16[128,384]{1,0:T(8,128)(2,1)}, bf16[128,384]{1,0:T(8,128)(2,1)S(1)}, u32[]{:S(2)}, u32[]{:S(2)}) collective-permute-start(bf16[128,384]{1,0:T(8,128)(2,1)} %get-tuple-element.32), channel_id=1, source_target_pairs={{0,24},{8,16},{16,8},{24,0},{1,25},{9,17},{17,9},{25,1},{2,26},{10... | collective-permute-start | bytes 294920 | tf_op jit(solution)/shard_map/ppermute | solution.py:72
  11.7 0.6 collective-permute-start.4
  12.3 3.3 %collective-permute-start.7 = (bf16[8,2048]{1,0:T(8,128)(2,1)}, bf16[8,2048]{1,0:T(8,128)(2,1)S(1)}, u32[]{:S(2)}, u32[]{:S(2)}) collective-permute-start(bf16[8,2048]{1,0:T(8,128)(2,1)} %get-tuple-element.33), channel_id=1, source_target_pairs={{0,8},{8,16},{16,24},{1,9},{9,17},{17,25},{2,10},{10,18},{18,26},{... | collective-permute-start | bytes 98312 | tf_op jit(solution)/shard_map/ppermute | solution.py:624
  15.9 1.6 %collective-permute-start.1 = (bf16[128,768]{1,0:T(8,128)(2,1)S(1)}, bf16[128,768]{1,0:T(8,128)(2,1)S(1)}, u32[]{:S(2)}, u32[]{:S(2)}) collective-permute-start(bf16[128,768]{1,0:T(8,128)(2,1)S(1)} %pad_maximum_fusion.2), channel_id=1, source_target_pairs={{0,2},{2,0},{4,6},{6,4},{1,3},{3,1},{5,7},{7,5},{8,10},{10,8},{12,... | collective-permute-start | bytes 589832 | tf_op jit(solution)/shard_map/ppermute | solution.py:72
  17.6 1.4 collective-permute-done.7
  19.0 1.5 %collective-permute-start.2 = (bf16[128,768]{1,0:T(8,128)(2,1)S(1)}, bf16[128,768]{1,0:T(8,128)(2,1)S(1)}, u32[]{:S(2)}, u32[]{:S(2)}) collective-permute-start(bf16[128,768]{1,0:T(8,128)(2,1)S(1)} %pad_maximum_fusion.3), channel_id=1, source_target_pairs={{0,4},{2,6},{4,0},{6,2},{1,5},{3,7},{5,1},{7,3},{8,12},{10,14},{12... | collective-permute-start | bytes 589832 | tf_op jit(solution)/shard_map/ppermute | solution.py:72
  20.6 1.5 collective-permute-start.3
  22.1 1.6 %collective-permute-start.20 = (bf16[128,2176]{1,0:T(8,128)(2,1)S(1)}, bf16[128,2176]{1,0:T(8,128)(2,1)}, u32[]{:S(2)}, u32[]{:S(2)}) collective-permute-start(bf16[128,2176]{1,0:T(8,128)(2,1)S(1)} %copy-done.5), channel_id=1, source_target_pairs={{0,6},{2,4},{4,2},{6,0},{1,7},{3,5},{5,3},{7,1},{8,14},{10,12},{12... | collective-permute-start | bytes 1671176 | tf_op jit(solution)/shard_map/ppermute | solution.py:72
  23.8 17.2 %collective-permute-done.2 = bf16[128,768]{1,0:T(8,128)(2,1)S(1)} collective-permute-done((bf16[128,768]{1,0:T(8,128)(2,1)S(1)}, bf16[128,768]{1,0:T(8,128)(2,1)S(1)}, u32[]{:S(2)}, u32[]{:S(2)}) %collective-permute-start.2) | collective-permute-done | bytes 196640 | tf_op jit(solution)/shard_map/ppermute | solution.py:72
  41.1 1.6 %collective-permute-start.11 = (bf16[560,384]{1,0:T(8,128)(2,1)S(1)}, bf16[560,384]{1,0:T(8,128)(2,1)S(1)}, u32[]{:S(2)}, u32[]{:S(2)}) collective-permute-start(bf16[560,384]{1,0:T(8,128)(2,1)S(1)} %maximum_dynamic-update-slice_fusion.refs_0_.refs_12_), channel_id=1, source_target_pairs={{0,4},{2,6},{4,0},{6,2},{1,5},{3,7},{5,1},{7,3},{8,12},{10,14},{12... | collective-permute-start | bytes 1290248 | tf_op jit(solution)/shard_map/ppermute | solution.py:72
  42.7 1.5 collective-permute-start.9
  44.1 7.3 %collective-permute-done.11.refs_4_.refs_16_ = bf16[560,384]{1,0:T(8,128)(2,1)S(1)} collective-permute-done((bf16[560,384]{1,0:T(8,128)(2,1)S(1)}, bf16[560,384]{1,0:T(8,128)(2,1)S(1)}, u32[]{:S(2)}, u32[]{:S(2)}) %collective-permute-start.11) | collective-permute-done | bytes 430112 | tf_op jit(solution)/shard_map/ppermute | solution.py:72
  51.5 1.6 %collective-permute-start.14 = (bf16[280,384]{1,0:T(8,128)(2,1)S(1)}, bf16[280,384]{1,0:T(8,128)(2,1)S(1)}, u32[]{:S(2)}, u32[]{:S(2)}) collective-permute-start(bf16[280,384]{1,0:T(8,128)(2,1)S(1)} %slice.14), channel_id=1, source_target_pairs={{0,2},{2,0},{4,6},{6,4},{1,3},{3,1},{5,7},{7,5},{8,10},{10,8},{12,... | collective-permute-start | bytes 645128 | tf_op jit(solution)/shard_map/ppermute | solution.py:72
  53.1 2.4 %collective-permute-start.22 = (bf16[512,768]{1,0:T(8,128)(2,1)S(1)}, bf16[512,768]{1,0:T(8,128)(2,1)}, u32[]{:S(2)}, u32[]{:S(2)}) collective-permute-start(bf16[512,768]{1,0:T(8,128)(2,1)S(1)} %pad_maximum_fusion.refs_8_), channel_id=1, source_target_pairs={{0,8},{8,16},{16,24},{24,0},{1,9},{9,17},{17,25},{25,1},{2,10},{10... | collective-permute-start | bytes 2359304 | tf_op jit(solution)/shard_map/ppermute | solution.py:84
  55.5 1.7 %collective-permute-start.18 = (bf16[128,2176]{1,0:T(8,128)(2,1)S(1)}, bf16[128,2176]{1,0:T(8,128)(2,1)}, u32[]{:S(2)}, u32[]{:S(2)}) collective-permute-start(bf16[128,2176]{1,0:T(8,128)(2,1)S(1)} %copy-done.5), channel_id=1, source_target_pairs={{0,4},{2,6},{4,0},{6,2},{1,5},{3,7},{5,1},{7,3},{8,12},{10,14},{12... | collective-permute-start | bytes 1671176 | tf_op jit(solution)/shard_map/ppermute | solution.py:72
  57.2 0.5 collective-permute-start.16
  57.8 0.5 collective-permute-done.14
  58.2 3.0 %collective-permute-start.13 = (bf16[280,384]{1,0:T(8,128)(2,1)S(1)}, bf16[280,384]{1,0:T(8,128)(2,1)S(1)}, u32[]{:S(2)}, u32[]{:S(2)}) collective-permute-start(bf16[280,384]{1,0:T(8,128)(2,1)S(1)} %slice.13), channel_id=1, source_target_pairs={{0,4},{2,6},{4,0},{6,2},{1,5},{3,7},{5,1},{7,3},{8,12},{10,14},{12... | collective-permute-start | bytes 645128 | tf_op jit(solution)/shard_map/ppermute | solution.py:72
  61.2 10.7 %collective-permute-done.13 = bf16[280,384]{1,0:T(8,128)(2,1)S(1)} collective-permute-done((bf16[280,384]{1,0:T(8,128)(2,1)S(1)}, bf16[280,384]{1,0:T(8,128)(2,1)S(1)}, u32[]{:S(2)}, u32[]{:S(2)}) %collective-permute-start.13) | collective-permute-done | bytes 215072 | tf_op jit(solution)/shard_map/ppermute | solution.py:72
  72.1 0.6 collective-permute-start.12
  72.6 0.1 collective-permute-start.10
  72.7 0.4 collective-permute-start.15
  73.2 0.6 collective-permute-done.8.refs_1_.refs_13_
  73.7 1.4 collective-permute-start.24
  75.2 0.6 collective-permute-start.23
  75.8 0.5 collective-permute-start.19
  76.3 0.3 copy-done.8
  76.6 0.2 copy-done.9
  76.7 0.3 collective-permute-start.17
  77.1 1.8 %copy.22 = bf16[256,512]{0,1:T(8,128)(2,1)} copy(bf16[256,512]{1,0:T(8,128)(2,1)} %param.27) | data formatting | bytes 524288 | tf_op args[7]
  78.9 4.2 %query.1 = (bf16[256,512]{1,0:T(8,128)(2,1)}, bf16[256,256]{1,0:T(8,128)(2,1)}) custom-call(s32[3]{0:T(128)} %pad_add_fusion.where_ref, bf16[128,2176]{1,0:T(8,128)(2,1)} %get-tuple-element.27.refs_0_, bf16[128,2176]{1,0:T(8,128)(2,1)} %copy-done.6, bf16[2048,768]{1,0:T(8,128)(2,1)} %refs_2_.1, f32[256,128]{1,0:T(8,128)} %get-tuple-element.72.cos_ref.refs_3_, ...), custom_call_target="tpu_custom_call" | custom-call | flops 1073741824 | bytes 1073741 | tf_op jit(solution)/shard_map/query/pallas_call | solution.py:657
  83.1 4.3 %attention.2 = (f32[4,1,256]{2,1,0:T(1,128)}, f32[4,1,256]{2,1,0:T(1,128)}, f32[4,128,256]{2,1,0:T(8,128)}) custom-call(s32[3]{0:T(128)} %pad_add_fusion.where_ref, bf16[256,512]{1,0:T(8,128)(2,1)} %get-tuple-element.28.plain_ref, bf16[256,256]{1,0:T(8,128)(2,1)} %get-tuple-element.29.turned_ref, bf16[256,512]{1,0:T(8,128)(2,1)} %ku_ref.3, ...), custom_call_target="tpu_custom_call" | custom-call | flops 3221225472 | bytes 3221225 | tf_op jit(solution)/shard_map/attention/pallas_call | solution.py:675
  87.4 6.0 %collective-permute-done.24.refs_11_ = bf16[512,768]{1,0:T(8,128)(2,1)} collective-permute-done((bf16[512,768]{1,0:T(8,128)(2,1)S(1)}, bf16[512,768]{1,0:T(8,128)(2,1)}, u32[]{:S(2)}, u32[]{:S(2)}) %collective-permute-start.24) | collective-permute-done | bytes 786464 | tf_op jit(solution)/shard_map/ppermute | solution.py:84
  93.4 17.7 %collective-permute-done.23.refs_10_ = bf16[512,768]{1,0:T(8,128)(2,1)} collective-permute-done((bf16[512,768]{1,0:T(8,128)(2,1)}, bf16[512,768]{1,0:T(8,128)(2,1)}, u32[]{:S(2)}, u32[]{:S(2)}) %collective-permute-start.23) | collective-permute-done | bytes 786464 | tf_op jit(solution)/shard_map/ppermute | solution.py:84
  111.1 13.2 %state_scan.1 = (f32[1024,256]{1,0:T(8,128)}, bf16[1024,128]{1,0:T(8,128)(2,1)}, bf16[1024,256]{1,0:T(8,128)(2,1)}, f32[1024,128]{1,0:T(8,128)}, bf16[144,256]{1,0:T(8,128)(2,1)}) custom-call(s32[3]{0:T(128)} %pad_add_fusion.where_ref, bf16[128,2176]{1,0:T(8,128)(2,1)} %get-tuple-element.27.refs_0_, bf16[128,2176]{1,0:T(8,128)(2,1)} %copy-done.6, ...), custom_call_target="tpu_custom_call" | custom-call | flops 4294967296 | bytes 4294967 | tf_op jit(solution)/shard_map/state_scan/pallas_call | solution.py:705
  124.3 2.0 %collective-permute-start.27 = (bf16[144,256]{1,0:T(8,128)(2,1)}, bf16[144,256]{1,0:T(8,128)(2,1)S(1)}, u32[]{:S(2)}, u32[]{:S(2)}) collective-permute-start(bf16[144,256]{1,0:T(8,128)(2,1)} %get-tuple-element.47), channel_id=1, source_target_pairs={{0,24},{8,16},{16,8},{24,0},{1,25},{9,17},{17,9},{25,1},{2,26},{10... | collective-permute-start | bytes 221192 | tf_op jit(solution)/shard_map/ppermute | solution.py:72
  126.3 0.2 collective-permute-start.26
  126.5 2.3 %collective-permute-start.25 = (bf16[144,256]{1,0:T(8,128)(2,1)}, bf16[144,256]{1,0:T(8,128)(2,1)S(1)}, u32[]{:S(2)}, u32[]{:S(2)}) collective-permute-start(bf16[144,256]{1,0:T(8,128)(2,1)} %get-tuple-element.47), channel_id=1, source_target_pairs={{0,8},{8,0},{16,24},{24,16},{1,9},{9,1},{17,25},{25,17},{2,10},{10... | collective-permute-start | bytes 221192 | tf_op jit(solution)/shard_map/ppermute | solution.py:72
  128.7 2.4 %attention.3 = bf16[256,512]{1,0:T(8,128)(2,1)} custom-call(s32[3]{0:T(128)} %pad_add_fusion.where_ref, bf16[256,512]{1,0:T(8,128)(2,1)} %get-tuple-element.28.plain_ref, bf16[256,256]{1,0:T(8,128)(2,1)} %get-tuple-element.29.turned_ref, bf16[256,512]{1,0:T(8,128)(2,1)} %ku_ref.3, bf16[512,256]{1,0:T(8,128)(2,1)} %bitcast.42, bf16[560,384]{1,0:T(8,128)(2,1)} %copy-done.4, ...), custom_call_target="tpu_custom_call" | custom-call | flops 1073741824 | bytes 1073741 | tf_op jit(solution)/shard_map/attention/pallas_call | solution.py:675
  131.2 0.1 collective-permute-done.27
  131.3 2.5 %collective-permute-done.26 = bf16[144,256]{1,0:T(8,128)(2,1)S(1)} collective-permute-done((bf16[144,256]{1,0:T(8,128)(2,1)}, bf16[144,256]{1,0:T(8,128)(2,1)S(1)}, u32[]{:S(2)}, u32[]{:S(2)}) %collective-permute-start.26) | collective-permute-done | bytes 73760 | tf_op jit(solution)/shard_map/ppermute | solution.py:72
  133.8 0.8 pad_maximum_fusion.1.states_ref
  134.5 4.3 %finish.1 = bf16[1024,256]{1,0:T(8,128)(2,1)} custom-call(s32[3]{0:T(128)} %pad_add_fusion.where_ref, bf16[4,144,256]{2,1,0:T(8,128)(2,1)} %pad_maximum_fusion.1.states_ref, f32[1024,256]{1,0:T(8,128)} %get-tuple-element.48.mixed_ref, bf16[1024,128]{1,0:T(8,128)(2,1)} %get-tuple-element.49.reads_ref, bf16[1024,256]{1,0:T(8,128)(2,1)} %get-tuple-element.50.gate_ref, ...), custom_call_target="tpu_custom_call" | custom-call | tf_op jit(solution)/shard_map/finish/pallas_call | solution.py:757
  138.9 12.0 %all_to_all.5 = bf16[4,256,256]{2,1,0:T(8,128)(2,1)S(1)} all-to-all(bf16[4,256,256]{2,1,0:T(8,128)(2,1)} %bitcast.40), channel_id=1, replica_groups=mesh['a'=4,'b'=4,'tp'=2] {'b'}, dimensions={0} | all-to-all | bytes 1048576 | tf_op jit(solution)/shard_map/all_to_all | solution.py:776
  150.9 0.9 copy.24
  (81 shorter events, 0.7 us)
Async XLA Ops:
  0.6 15.1 %copy-start.12 = (bf16[128,1024]{1,0:T(8,128)(2,1)S(1)}, bf16[128,1024]{1,0:T(8,128)(2,1)}, u32[]{:S(2)}) copy-start(bf16[128,1024]{1,0:T(8,128)(2,1)} %param.28) | copy-start | bytes 786436
  0.6 15.0 %copy-start.11 = (bf16[128,1024]{1,0:T(8,128)(2,1)S(1)}, bf16[128,1024]{1,0:T(8,128)(2,1)}, u32[]{:S(2)}) copy-start(bf16[128,1024]{1,0:T(8,128)(2,1)} %param.29) | copy-start | bytes 786436
  2.7 13.1 %copy-start.13 = (bf16[128,512]{1,0:T(8,128)(2,1)S(1)}, bf16[128,512]{1,0:T(8,128)(2,1)}, u32[]{:S(2)}) copy-start(bf16[128,512]{1,0:T(8,128)(2,1)} %param.31) | copy-start | bytes 393220
  2.7 13.1 %copy-start.14 = (bf16[128,512]{1,0:T(8,128)(2,1)S(1)}, bf16[128,512]{1,0:T(8,128)(2,1)}, u32[]{:S(2)}) copy-start(bf16[128,512]{1,0:T(8,128)(2,1)} %param.30) | copy-start | bytes 393220
  6.5 11.0 %copy-start.15 = (bf16[128,384]{1,0:T(8,128)(2,1)S(1)}, bf16[128,384]{1,0:T(8,128)(2,1)}, u32[]{:S(2)}) copy-start(bf16[128,384]{1,0:T(8,128)(2,1)} %get-tuple-element.32) | copy-start | bytes 294916
  6.5 11.0 %copy-start.17 = (f32[256,16]{0,1:T(8,128)S(1)}, f32[256,16]{0,1:T(8,128)}, u32[]{:S(2)}) copy-start(f32[256,16]{0,1:T(8,128)} %param.37) | copy-start | bytes 49156
  6.5 17.2 %collective-permute-start.6 = (bf16[128,384]{1,0:T(8,128)(2,1)}, bf16[128,384]{1,0:T(8,128)(2,1)S(1)}, u32[]{:S(2)}, u32[]{:S(2)}) collective-permute-start(bf16[128,384]{1,0:T(8,128)(2,1)} %get-tuple-element.32), channel_id=1, source_target_pairs={{0,24},{8,16},{16,8},{24,0},{1,25},{9,17},{17,9},{25,1},{2,26},{10... | collective-permute-start | bytes 294920 | tf_op jit(solution)/shard_map/ppermute | solution.py:72
  11.7 10.4 %collective-permute-start.5 = (bf16[128,384]{1,0:T(8,128)(2,1)}, bf16[128,384]{1,0:T(8,128)(2,1)S(1)}, u32[]{:S(2)}, u32[]{:S(2)}) collective-permute-start(bf16[128,384]{1,0:T(8,128)(2,1)} %get-tuple-element.32), channel_id=1, source_target_pairs={{0,16},{8,24},{16,0},{24,8},{1,17},{9,25},{17,1},{25,9},{2,18},{10... | collective-permute-start | bytes 294920 | tf_op jit(solution)/shard_map/ppermute | solution.py:72
  11.7 8.9 %collective-permute-start.4 = (bf16[128,384]{1,0:T(8,128)(2,1)}, bf16[128,384]{1,0:T(8,128)(2,1)S(1)}, u32[]{:S(2)}, u32[]{:S(2)}) collective-permute-start(bf16[128,384]{1,0:T(8,128)(2,1)} %get-tuple-element.32), channel_id=1, source_target_pairs={{0,8},{8,0},{16,24},{24,16},{1,9},{9,1},{17,25},{25,17},{2,10},{10... | collective-permute-start | bytes 294920 | tf_op jit(solution)/shard_map/ppermute | solution.py:72
  12.3 6.7 %collective-permute-start.7 = (bf16[8,2048]{1,0:T(8,128)(2,1)}, bf16[8,2048]{1,0:T(8,128)(2,1)S(1)}, u32[]{:S(2)}, u32[]{:S(2)}) collective-permute-start(bf16[8,2048]{1,0:T(8,128)(2,1)} %get-tuple-element.33), channel_id=1, source_target_pairs={{0,8},{8,16},{16,24},{1,9},{9,17},{17,25},{2,10},{10,18},{18,26},{... | collective-permute-start | bytes 98312 | tf_op jit(solution)/shard_map/ppermute | solution.py:624
  15.7 6.5 %copy-start.5 = (bf16[128,2176]{1,0:T(8,128)(2,1)S(1)}, bf16[128,2176]{1,0:T(8,128)(2,1)}, u32[]{:S(2)}) copy-start(bf16[128,2176]{1,0:T(8,128)(2,1)} %get-tuple-element.27.refs_0_) | copy-start | bytes 1671172
  15.9 7.9 %collective-permute-start.1 = (bf16[128,768]{1,0:T(8,128)(2,1)S(1)}, bf16[128,768]{1,0:T(8,128)(2,1)S(1)}, u32[]{:S(2)}, u32[]{:S(2)}) collective-permute-start(bf16[128,768]{1,0:T(8,128)(2,1)S(1)} %pad_maximum_fusion.2), channel_id=1, source_target_pairs={{0,2},{2,0},{4,6},{6,4},{1,3},{3,1},{5,7},{7,5},{8,10},{10,8},{12,... | collective-permute-start | bytes 589832 | tf_op jit(solution)/shard_map/ppermute | solution.py:72
  19.0 22.0 %collective-permute-start.2 = (bf16[128,768]{1,0:T(8,128)(2,1)S(1)}, bf16[128,768]{1,0:T(8,128)(2,1)S(1)}, u32[]{:S(2)}, u32[]{:S(2)}) collective-permute-start(bf16[128,768]{1,0:T(8,128)(2,1)S(1)} %pad_maximum_fusion.3), channel_id=1, source_target_pairs={{0,4},{2,6},{4,0},{6,2},{1,5},{3,7},{5,1},{7,3},{8,12},{10,14},{12... | collective-permute-start | bytes 589832 | tf_op jit(solution)/shard_map/ppermute | solution.py:72
  20.6 20.4 %collective-permute-start.3 = (bf16[128,768]{1,0:T(8,128)(2,1)S(1)}, bf16[128,768]{1,0:T(8,128)(2,1)S(1)}, u32[]{:S(2)}, u32[]{:S(2)}) collective-permute-start(bf16[128,768]{1,0:T(8,128)(2,1)S(1)} %pad_maximum_fusion.4), channel_id=1, source_target_pairs={{0,6},{2,4},{4,2},{6,0},{1,7},{3,5},{5,3},{7,1},{8,14},{10,12},{12... | collective-permute-start | bytes 589832 | tf_op jit(solution)/shard_map/ppermute | solution.py:72
  22.1 35.1 %collective-permute-start.20 = (bf16[128,2176]{1,0:T(8,128)(2,1)S(1)}, bf16[128,2176]{1,0:T(8,128)(2,1)}, u32[]{:S(2)}, u32[]{:S(2)}) collective-permute-start(bf16[128,2176]{1,0:T(8,128)(2,1)S(1)} %copy-done.5), channel_id=1, source_target_pairs={{0,6},{2,4},{4,2},{6,0},{1,7},{3,5},{5,3},{7,1},{8,14},{10,12},{12... | collective-permute-start | bytes 1671176 | tf_op jit(solution)/shard_map/ppermute | solution.py:72
  23.8 48.3 %copy-start.4 = (bf16[560,384]{1,0:T(8,128)(2,1)}, bf16[560,384]{1,0:T(8,128)(2,1)S(1)}, u32[]{:S(2)}) copy-start(bf16[560,384]{1,0:T(8,128)(2,1)S(1)} %maximum_dynamic-update-slice_fusion.refs_0_.refs_12_) | copy-start | bytes 1290244
  41.1 42.0 %copy-start.3 = (bf16[512,768]{1,0:T(8,128)(2,1)}, bf16[512,768]{1,0:T(8,128)(2,1)S(1)}, u32[]{:S(2)}) copy-start(bf16[512,768]{1,0:T(8,128)(2,1)S(1)} %pad_maximum_fusion.refs_8_) | copy-start | bytes 2359300
  41.1 10.4 %collective-permute-start.11 = (bf16[560,384]{1,0:T(8,128)(2,1)S(1)}, bf16[560,384]{1,0:T(8,128)(2,1)S(1)}, u32[]{:S(2)}, u32[]{:S(2)}) collective-permute-start(bf16[560,384]{1,0:T(8,128)(2,1)S(1)} %maximum_dynamic-update-slice_fusion.refs_0_.refs_12_), channel_id=1, source_target_pairs={{0,4},{2,6},{4,0},{6,2},{1,5},{3,7},{5,1},{7,3},{8,12},{10,14},{12... | collective-permute-start | bytes 1290248 | tf_op jit(solution)/shard_map/ppermute | solution.py:72
  42.7 15.1 %collective-permute-start.9 = (bf16[560,384]{1,0:T(8,128)(2,1)S(1)}, bf16[560,384]{1,0:T(8,128)(2,1)S(1)}, u32[]{:S(2)}, u32[]{:S(2)}) collective-permute-start(bf16[560,384]{1,0:T(8,128)(2,1)S(1)} %maximum_dynamic-update-slice_fusion.refs_0_.refs_12_), channel_id=1, source_target_pairs={{0,2},{2,0},{4,6},{6,4},{1,3},{3,1},{5,7},{7,5},{8,10},{10,8},{12,... | collective-permute-start | bytes 1290248 | tf_op jit(solution)/shard_map/ppermute | solution.py:72
  51.5 31.5 %copy-start = (bf16[560,384]{1,0:T(8,128)(2,1)}, bf16[560,384]{1,0:T(8,128)(2,1)S(1)}, u32[]{:S(2)}) copy-start(bf16[560,384]{1,0:T(8,128)(2,1)S(1)} %collective-permute-done.11.refs_4_.refs_16_) | copy-start | bytes 1290244
  51.5 6.7 %collective-permute-start.14 = (bf16[280,384]{1,0:T(8,128)(2,1)S(1)}, bf16[280,384]{1,0:T(8,128)(2,1)S(1)}, u32[]{:S(2)}, u32[]{:S(2)}) collective-permute-start(bf16[280,384]{1,0:T(8,128)(2,1)S(1)} %slice.14), channel_id=1, source_target_pairs={{0,2},{2,0},{4,6},{6,4},{1,3},{3,1},{5,7},{7,5},{8,10},{10,8},{12,... | collective-permute-start | bytes 645128 | tf_op jit(solution)/shard_map/ppermute | solution.py:72
  53.1 22.1 %collective-permute-start.22 = (bf16[512,768]{1,0:T(8,128)(2,1)S(1)}, bf16[512,768]{1,0:T(8,128)(2,1)}, u32[]{:S(2)}, u32[]{:S(2)}) collective-permute-start(bf16[512,768]{1,0:T(8,128)(2,1)S(1)} %pad_maximum_fusion.refs_8_), channel_id=1, source_target_pairs={{0,8},{8,16},{16,24},{24,0},{1,9},{9,17},{17,25},{25,1},{2,10},{10... | collective-permute-start | bytes 2359304 | tf_op jit(solution)/shard_map/ppermute | solution.py:84
  55.5 16.6 %collective-permute-start.18 = (bf16[128,2176]{1,0:T(8,128)(2,1)S(1)}, bf16[128,2176]{1,0:T(8,128)(2,1)}, u32[]{:S(2)}, u32[]{:S(2)}) collective-permute-start(bf16[128,2176]{1,0:T(8,128)(2,1)S(1)} %copy-done.5), channel_id=1, source_target_pairs={{0,4},{2,6},{4,0},{6,2},{1,5},{3,7},{5,1},{7,3},{8,12},{10,14},{12... | collective-permute-start | bytes 1671176 | tf_op jit(solution)/shard_map/ppermute | solution.py:72
  57.2 15.4 %collective-permute-start.16 = (bf16[128,2176]{1,0:T(8,128)(2,1)S(1)}, bf16[128,2176]{1,0:T(8,128)(2,1)}, u32[]{:S(2)}, u32[]{:S(2)}) collective-permute-start(bf16[128,2176]{1,0:T(8,128)(2,1)S(1)} %copy-done.5), channel_id=1, source_target_pairs={{0,2},{2,0},{4,6},{6,4},{1,3},{3,1},{5,7},{7,5},{8,10},{10,8},{12,... | collective-permute-start | bytes 1671176 | tf_op jit(solution)/shard_map/ppermute | solution.py:72
  57.7 25.3 %copy-start.1 = (bf16[560,384]{1,0:T(8,128)(2,1)}, bf16[560,384]{1,0:T(8,128)(2,1)S(1)}, u32[]{:S(2)}) copy-start(bf16[560,384]{1,0:T(8,128)(2,1)S(1)} %collective-permute-done.9.refs_2_.refs_14_) | copy-start | bytes 1290244
  57.7 15.0 %collective-permute-start = (bf16[128,2176]{1,0:T(8,128)(2,1)S(1)}, bf16[128,2176]{1,0:T(8,128)(2,1)S(1)}, u32[]{:S(2)}, u32[]{:S(2)}) collective-permute-start(bf16[128,2176]{1,0:T(8,128)(2,1)S(1)} %copy-done.5), channel_id=1, source_target_pairs={{0,1},{1,0},{2,3},{3,2},{4,5},{5,4},{6,7},{7,6},{8,9},{9,8},{10,11... | collective-permute-start | bytes 1671176 | tf_op jit(solution)/shard_map/ppermute | solution.py:72
  58.2 13.7 %collective-permute-start.13 = (bf16[280,384]{1,0:T(8,128)(2,1)S(1)}, bf16[280,384]{1,0:T(8,128)(2,1)S(1)}, u32[]{:S(2)}, u32[]{:S(2)}) collective-permute-start(bf16[280,384]{1,0:T(8,128)(2,1)S(1)} %slice.13), channel_id=1, source_target_pairs={{0,4},{2,6},{4,0},{6,2},{1,5},{3,7},{5,1},{7,3},{8,12},{10,14},{12... | collective-permute-start | bytes 645128 | tf_op jit(solution)/shard_map/ppermute | solution.py:72
  72.0 1.8 %collective-permute-start.8 = (bf16[560,384]{1,0:T(8,128)(2,1)S(1)}, bf16[560,384]{1,0:T(8,128)(2,1)S(1)}, u32[]{:S(2)}, u32[]{:S(2)}) collective-permute-start(bf16[560,384]{1,0:T(8,128)(2,1)S(1)} %maximum_dynamic-update-slice_fusion.refs_0_.refs_12_), channel_id=1, source_target_pairs={{0,1},{1,0},{2,3},{3,2},{4,5},{5,4},{6,7},{7,6},{8,9},{9,8},{10,11... | collective-permute-start | bytes 1290248 | tf_op jit(solution)/shard_map/ppermute | solution.py:72
  72.0 11.0 %copy-start.2 = (bf16[560,384]{1,0:T(8,128)(2,1)}, bf16[560,384]{1,0:T(8,128)(2,1)S(1)}, u32[]{:S(2)}) copy-start(bf16[560,384]{1,0:T(8,128)(2,1)S(1)} %constant_dynamic-update-slice_fusion.4.refs_6_.refs_18_) | copy-start | bytes 1290244
  72.1 3.7 %collective-permute-start.12 = (bf16[560,384]{1,0:T(8,128)(2,1)S(1)}, bf16[560,384]{1,0:T(8,128)(2,1)S(1)}, u32[]{:S(2)}, u32[]{:S(2)}) collective-permute-start(bf16[560,384]{1,0:T(8,128)(2,1)S(1)} %collective-permute-done.11.refs_4_.refs_16_), channel_id=1, source_target_pairs={{0,1},{1,0},{2,3},{3,2},{4,5},{5,4},{6,7},{7,6},{8,9},{9,8},{10,11... | collective-permute-start | bytes 1290248 | tf_op jit(solution)/shard_map/ppermute | solution.py:72
  72.6 3.1 %collective-permute-start.10 = (bf16[560,384]{1,0:T(8,128)(2,1)S(1)}, bf16[560,384]{1,0:T(8,128)(2,1)S(1)}, u32[]{:S(2)}, u32[]{:S(2)}) collective-permute-start(bf16[560,384]{1,0:T(8,128)(2,1)S(1)} %collective-permute-done.9.refs_2_.refs_14_), channel_id=1, source_target_pairs={{0,1},{1,0},{2,3},{3,2},{4,5},{5,4},{6,7},{7,6},{8,9},{9,8},{10,11... | collective-permute-start | bytes 1290248 | tf_op jit(solution)/shard_map/ppermute | solution.py:72
  72.7 3.6 %copy-start.6 = (bf16[128,2176]{1,0:T(8,128)(2,1)}, bf16[128,2176]{1,0:T(8,128)(2,1)S(1)}, u32[]{:S(2)}) copy-start(bf16[128,2176]{1,0:T(8,128)(2,1)S(1)} %collective-permute-done.refs_1_) | copy-start | bytes 1671172
  72.7 3.6 %collective-permute-start.15 = (bf16[560,384]{1,0:T(8,128)(2,1)S(1)}, bf16[560,384]{1,0:T(8,128)(2,1)S(1)}, u32[]{:S(2)}, u32[]{:S(2)}) collective-permute-start(bf16[560,384]{1,0:T(8,128)(2,1)S(1)} %constant_dynamic-update-slice_fusion.4.refs_6_.refs_18_), channel_id=1, source_target_pairs={{0,1},{1,0},{2,3},{3,2},{4,5},{5,4},{6,7},{7,6},{8,9},{9,8},{10,11... | collective-permute-start | bytes 1290248 | tf_op jit(solution)/shard_map/ppermute | solution.py:72
  73.7 9.3 %copy-start.7 = (bf16[560,384]{1,0:T(8,128)(2,1)}, bf16[560,384]{1,0:T(8,128)(2,1)S(1)}, u32[]{:S(2)}) copy-start(bf16[560,384]{1,0:T(8,128)(2,1)S(1)} %collective-permute-done.8.refs_1_.refs_13_) | copy-start | bytes 1290244
  73.7 19.7 %collective-permute-start.24 = (bf16[512,768]{1,0:T(8,128)(2,1)S(1)}, bf16[512,768]{1,0:T(8,128)(2,1)}, u32[]{:S(2)}, u32[]{:S(2)}) collective-permute-start(bf16[512,768]{1,0:T(8,128)(2,1)S(1)} %pad_maximum_fusion.refs_8_), channel_id=1, source_target_pairs={{0,24},{8,0},{16,8},{24,16},{1,25},{9,1},{17,9},{25,17},{2,26},{10... | collective-permute-start | bytes 2359304 | tf_op jit(solution)/shard_map/ppermute | solution.py:84
  75.2 35.9 %collective-permute-start.23 = (bf16[512,768]{1,0:T(8,128)(2,1)}, bf16[512,768]{1,0:T(8,128)(2,1)}, u32[]{:S(2)}, u32[]{:S(2)}) collective-permute-start(bf16[512,768]{1,0:T(8,128)(2,1)} %collective-permute-done.22.refs_9_), channel_id=1, source_target_pairs={{0,8},{8,16},{16,24},{24,0},{1,9},{9,17},{17,25},{25,1},{2,10},{10... | collective-permute-start | bytes 2359304 | tf_op jit(solution)/shard_map/ppermute | solution.py:84
  75.8 0.8 copy-start.8
  75.8 17.7 %collective-permute-start.21 = (bf16[128,2176]{1,0:T(8,128)(2,1)}, bf16[128,2176]{1,0:T(8,128)(2,1)}, u32[]{:S(2)}, u32[]{:S(2)}) collective-permute-start(bf16[128,2176]{1,0:T(8,128)(2,1)} %collective-permute-done.20.refs_6_), channel_id=1, source_target_pairs={{0,1},{1,0},{2,3},{3,2},{4,5},{5,4},{6,7},{7,6},{8,9},{9,8},{10,11... | collective-permute-start | bytes 1671176 | tf_op jit(solution)/shard_map/ppermute | solution.py:72
  75.8 0.9 copy-start.9
  75.8 17.6 %collective-permute-start.19 = (bf16[128,2176]{1,0:T(8,128)(2,1)}, bf16[128,2176]{1,0:T(8,128)(2,1)}, u32[]{:S(2)}, u32[]{:S(2)}) collective-permute-start(bf16[128,2176]{1,0:T(8,128)(2,1)} %collective-permute-done.18.refs_4_), channel_id=1, source_target_pairs={{0,1},{1,0},{2,3},{3,2},{4,5},{5,4},{6,7},{7,6},{8,9},{9,8},{10,11... | collective-permute-start | bytes 1671176 | tf_op jit(solution)/shard_map/ppermute | solution.py:72
  76.7 6.3 %copy-start.10 = (bf16[560,384]{1,0:T(8,128)(2,1)}, bf16[560,384]{1,0:T(8,128)(2,1)S(1)}, u32[]{:S(2)}) copy-start(bf16[560,384]{1,0:T(8,128)(2,1)S(1)} %collective-permute-done.15.refs_7_.refs_19_) | copy-start | bytes 1290244
  76.7 16.7 %collective-permute-start.17 = (bf16[128,2176]{1,0:T(8,128)(2,1)}, bf16[128,2176]{1,0:T(8,128)(2,1)}, u32[]{:S(2)}, u32[]{:S(2)}) collective-permute-start(bf16[128,2176]{1,0:T(8,128)(2,1)} %collective-permute-done.16.refs_2_), channel_id=1, source_target_pairs={{0,1},{1,0},{2,3},{3,2},{4,5},{5,4},{6,7},{7,6},{8,9},{9,8},{10,11... | collective-permute-start | bytes 1671176 | tf_op jit(solution)/shard_map/ppermute | solution.py:72
  124.3 7.0 %collective-permute-start.27 = (bf16[144,256]{1,0:T(8,128)(2,1)}, bf16[144,256]{1,0:T(8,128)(2,1)S(1)}, u32[]{:S(2)}, u32[]{:S(2)}) collective-permute-start(bf16[144,256]{1,0:T(8,128)(2,1)} %get-tuple-element.47), channel_id=1, source_target_pairs={{0,24},{8,16},{16,8},{24,0},{1,25},{9,17},{17,9},{25,1},{2,26},{10... | collective-permute-start | bytes 221192 | tf_op jit(solution)/shard_map/ppermute | solution.py:72
  126.3 7.4 %collective-permute-start.26 = (bf16[144,256]{1,0:T(8,128)(2,1)}, bf16[144,256]{1,0:T(8,128)(2,1)S(1)}, u32[]{:S(2)}, u32[]{:S(2)}) collective-permute-start(bf16[144,256]{1,0:T(8,128)(2,1)} %get-tuple-element.47), channel_id=1, source_target_pairs={{0,16},{8,24},{16,0},{24,8},{1,17},{9,25},{17,1},{25,9},{2,18},{10... | collective-permute-start | bytes 221192 | tf_op jit(solution)/shard_map/ppermute | solution.py:72
  126.5 7.3 %collective-permute-start.25 = (bf16[144,256]{1,0:T(8,128)(2,1)}, bf16[144,256]{1,0:T(8,128)(2,1)S(1)}, u32[]{:S(2)}, u32[]{:S(2)}) collective-permute-start(bf16[144,256]{1,0:T(8,128)(2,1)} %get-tuple-element.47), channel_id=1, source_target_pairs={{0,8},{8,0},{16,24},{24,16},{1,9},{9,1},{17,25},{25,17},{2,10},{10... | collective-permute-start | bytes 221192 | tf_op jit(solution)/shard_map/ppermute | solution.py:72
  128.7 5.0 %copy-start.16 = (bf16[144,256]{1,0:T(8,128)(2,1)S(1)}, bf16[144,256]{1,0:T(8,128)(2,1)}, u32[]{:S(2)}) copy-start(bf16[144,256]{1,0:T(8,128)(2,1)} %get-tuple-element.47) | copy-start | bytes 221188

commit v2 on v1

--- a/solution.py
+++ b/solution.py
@@ -322,7 +322,6 @@
         skip_ref,
         mixed_ref,
         reads_ref,
-        gate_ref,
         run_ref,
         state_ref,
         xs,
@@ -339,7 +338,6 @@
     ia, ib, it = where_ref[0], where_ref[1], where_ref[2]
     deep = ws_in[0].shape[0]
     channels = heads * SSM_DIM
-    conv = channels + 2 * SSM_STATE
     span = ci_ref.shape[0]
     bottom = tails_in[0].shape[0] - tails.shape[1]
     for k in range(planes):
@@ -365,6 +363,7 @@
         pltpu.make_async_copy(tails.at[k], tails.at[k], tsem.at[k]).wait()
     pltpu.make_async_copy(tails.at[planes], tails.at[planes], tsem.at[planes]).wait()
     edge = tails[planes, :, length:].astype(f32)
+    edge = jnp.where(ia > 0, edge, jnp.zeros_like(edge))
     hx[...] = jnp.zeros(hx.shape, f32)
     each = edge.shape[0] // (span - 1)
     for r in range(span - 1):
@@ -412,14 +411,13 @@
     )
     for k in range(weights):
         pltpu.make_async_copy(ws_in[k], ws.at[pl.ds(0, deep), :], wsem.at[k]).wait()
-    raws[0, 0:8, :] = nn(hx[...].astype(bf16), ws[:, :conv]).astype(bf16).astype(f32)
+    raws[0, 0:8, :] = nn(hx[...].astype(bf16), ws[...]).astype(bf16).astype(f32)
 
     def product(c):
         here = pl.ds(c * length, length)
         pltpu.make_async_copy(xs.at[here, :], xs.at[here, :], xsem.at[c]).wait()
         raw = nn(xs[here, :model], ws[...]).astype(bf16)
-        gate_ref[here, :] = raw[:, conv:]
-        raw = raw[:, :conv].astype(f32)
+        raw = raw.astype(f32)
         raws[c, 8:, :] = raw
         if c + 1 < planes:
             raws[c + 1, 0:8, :] = raw[length - 8 :, :]
@@ -484,9 +482,41 @@
     state_ref[SSM_STATE :, :] = tail
 
 
-def finish_kernel(
-    where_ref, states_ref, mixed_ref, reads_ref, gate_ref, run_ref, gain_ref, out_ref, into_s, *, heads
-):
+def gate_kernel(where_ref, *refs, parts, planes, cores, weights, length):
+    nx = len(parts)
+    xs_in = refs[:nx]
+    ws_in = refs[nx : nx + weights]
+    out_ref, xs, ws, xsem, wsem = refs[nx + weights :]
+    ia = where_ref[0]
+    deep = ws_in[0].shape[0]
+    model = ws.shape[0]
+
+    for k in range(weights):
+        for copy in weight_copies(
+            where_ref, ws_in[k], ia ^ k, ws, wsem.at[k], planes
+        ):
+            copy.start()
+    for copy in row_copies(where_ref, xs_in, parts, xs, xsem, length, cores, model):
+        copy.start()
+    for k in range(weights):
+        pltpu.make_async_copy(ws_in[k], ws.at[pl.ds(0, deep), :], wsem.at[k]).wait()
+    batch = 2 if planes % 2 == 0 else 1
+
+    def some(c, carry):
+        for i in range(batch):
+            block = c * batch + i
+            at = pl.ds(pl.multiple_of(block * length, length), length)
+            pltpu.make_async_copy(xs.at[at, :], xs.at[at, :], xsem.at[block]).wait()
+        here = pl.ds(pl.multiple_of(c * batch * length, batch * length), batch * length)
+        out_ref[here, :] = nn(xs[here, :], ws[...]).astype(bf16)
+        return carry
+
+    lax.fori_loop(0, planes // batch, some, 0)
+
+
+def finish_kernel(where_ref, *refs, heads, planes):
+    states, refs = refs[: len(refs) - 7], refs[len(refs) - 7 :]
+    mixed_ref, reads_ref, gate_ref, run_ref, gain_ref, out_ref, into_s = refs
     here = where_ref[0]
     rows = mixed_ref.shape[0]
     channels = mixed_ref.shape[1]
@@ -495,17 +525,24 @@
     def _():
         into_s[...] = jnp.zeros(into_s.shape, f32)
 
-        def add(j, carry):
-            piece = states_ref[here ^ j].astype(f32)
-            decay = jnp.exp(
-                piece[SSM_STATE : SSM_STATE + 1]
-                + piece[SSM_STATE + 1 : SSM_STATE + 2]
-                + piece[SSM_STATE + 2 : SSM_STATE + 3]
-            )
-            into_s[...] = into_s[...] * decay + piece[:SSM_STATE]
+        def add(piece):
+            piece = piece.astype(f32)
+            total = piece[SSM_STATE : SSM_STATE + 3].sum(axis=0, keepdims=True)
+            into_s[...] = into_s[...] * jnp.exp(total) + piece[:SSM_STATE]
+
+        def stacked(j, carry):
+            add(states[0][here ^ j])
             return carry
 
-        lax.fori_loop(0, here, add, 0)
+        if len(states) == 1:
+            lax.fori_loop(0, here, stacked, 0)
+        else:
+            for j in range(planes - 1):
+                for k in range(planes):
+
+                    @pl.when((j < here) & ((here ^ k) == j))
+                    def _():
+                        add(states[k][...])
 
     lane = lax.broadcasted_iota(jnp.int32, (rows, LANES), 1)
     reach = jnp.exp(wide_heads(run_ref[...], heads, lane))
@@ -619,9 +656,11 @@
             (scan_gate, channels),
         ],
     )
-    packed = jnp.concatenate(packed, axis=0)
-
-    edge = lax.ppermute(edge, "a", [(i, i + 1) for i in range(A - 1)])
+    conv = channels + 2 * SSM_STATE
+    gating = jnp.concatenate([piece[:, conv:] for piece in packed], axis=0)
+    packed = jnp.concatenate([piece[:, :conv] for piece in packed], axis=0)
+
+    edge = lax.ppermute(edge, "a", [(i, (i + 1) % A) for i in range(A)])
     edge = edge[8 - taps + 1 :].reshape(-1, LANES)
     offsets = three_parts(decay_offset.T).reshape(3 * local, length)
     offsets = jnp.pad(offsets, ((0, edge.shape[0] - 3 * local), (0, 0)))
@@ -629,6 +668,8 @@
     key_stack = jnp.concatenate(exchange(key_own, "a") + [tail], axis=0)
     packed, key_stack = lax.optimization_barrier((packed, key_stack))
     w_pieces = ring(packed, "a")
+    gating, w_pieces[0] = lax.optimization_barrier((gating, w_pieces[0]))
+    g_pieces = exchange(gating, "a")
     key_pieces = []
     if B == 4:
         kside, kfront = across(key_stack, "b", 1), across(key_stack, "b", 2)
@@ -697,12 +738,11 @@
             name="attention",
         )(place, plain, turned, key_up, value_t, *key_pieces, *carry)
 
-    first_part = (3 * A * B) // 4
+    first_part = (5 * A * B) // 8
     carry = attend(where, 0, first_part, ())
     then, carry = lax.optimization_barrier((where, carry))
 
-    conv = channels + 2 * SSM_STATE
-    mixed, reads, gate, run, state = pl.pallas_call(
+    mixed, reads, run, state = pl.pallas_call(
         functools.partial(
             scan_kernel,
             parts=tuple(parts),
@@ -714,17 +754,16 @@
             every=every,
         ),
         in_specs=[smem()] + [hbm()] * (len(parts) + A + B * T) + [vmem()] * 5,
-        out_specs=[vmem()] * 5,
+        out_specs=[vmem()] * 4,
         out_shape=(
             shape((span, channels), f32),
             shape((span, SSM_STATE), bf16),
-            shape((span, channels), bf16),
             shape((span, LANES), f32),
             shape((SSM_STATE + SSM_STATE // 8, channels), bf16),
         ),
         scratch_shapes=[
             pltpu.VMEM((span, model + LANES), bf16),
-            pltpu.VMEM((model, conv + channels), bf16),
+            pltpu.VMEM((model, conv), bf16),
             pltpu.VMEM((8, model), f32),
             pltpu.VMEM((B, 8 + length, conv), f32),
             pltpu.VMEM((SSM_STATE, channels), f32),
@@ -749,29 +788,51 @@
         skip_gain.reshape(1, -1),
     )
 
-    states = jnp.stack(exchange(state, "a"))
+    states = exchange(state, "a")
+    if A > DIRECT:
+        states = [jnp.stack(states)]
     then, mixed = lax.optimization_barrier((then, mixed))
-    (attended,) = attend(then, first_part, A * B, carry)
-    gate, attended = lax.optimization_barrier((gate, attended))
+    gate = pl.pallas_call(
+        functools.partial(
+            gate_kernel, parts=tuple(parts), planes=B, cores=T, weights=A, length=length
+        ),
+        in_specs=[smem()] + [hbm()] * (len(parts) + A),
+        out_specs=vmem(),
+        out_shape=shape((span, channels), bf16),
+        scratch_shapes=[
+            pltpu.VMEM((span, model), bf16),
+            pltpu.VMEM((model, channels), bf16),
+            pltpu.SemaphoreType.DMA((B,)),
+            pltpu.SemaphoreType.DMA((A,)),
+        ],
+        compiler_params=params(),
+        cost_estimate=cost(2 * span * model * channels),
+        name="gate",
+    )(then, *x_pieces, *g_pieces)
 
     scanned = pl.pallas_call(
-        functools.partial(finish_kernel, heads=per_group),
-        grid=(B,),
+        functools.partial(finish_kernel, heads=per_group, planes=A),
+        grid=(2,),
         in_specs=[
             smem(),
-            pl.BlockSpec(states.shape, lambda i: (0, 0, 0)),
-            pl.BlockSpec((length, channels), lambda i: (i, 0)),
-            pl.BlockSpec((length, SSM_STATE), lambda i: (i, 0)),
-            pl.BlockSpec((length, channels), lambda i: (i, 0)),
-            pl.BlockSpec((length, LANES), lambda i: (i, 0)),
+            *[
+                pl.BlockSpec(piece.shape, lambda i, rank=piece.ndim: (0,) * rank)
+                for piece in states
+            ],
+            pl.BlockSpec((span // 2, channels), lambda i: (i, 0)),
+            pl.BlockSpec((span // 2, SSM_STATE), lambda i: (i, 0)),
+            pl.BlockSpec((span // 2, channels), lambda i: (i, 0)),
+            pl.BlockSpec((span // 2, LANES), lambda i: (i, 0)),
             pl.BlockSpec((1, group_gain.shape[0]), lambda i: (0, 0)),
         ],
-        out_specs=pl.BlockSpec((length, channels), lambda i: (i, 0)),
+        out_specs=pl.BlockSpec((span // 2, channels), lambda i: (i, 0)),
         out_shape=shape((span, channels), bf16),
         scratch_shapes=[pltpu.VMEM((SSM_STATE, channels), f32)],
         compiler_params=params(),
         name="finish",
-    )(where, states, mixed, reads, gate, run, group_gain.reshape(1, -1))
+    )(where, *states, mixed, reads, gate, run, group_gain.reshape(1, -1))
+    last, scanned = lax.optimization_barrier((then, scanned))
+    (attended,) = attend(last, first_part, A * B, carry)
     if B > 1:
         scanned = lax.all_to_all(scanned.reshape(B, length, channels), "b", 0, 0, tiled=True)
         scanned = jnp.transpose(scanned, (1, 0, 2)).reshape(length, B * channels)

time: 152 us -> 166 us (1.092)
  the two profiles are of different devices: /device:TPU:0 before, /device:TPU:8 now
where the time goes in v2:
time: 166 us; the launch traced here: 165 us
  waiting for transfers between devices  68.4 us (41%)
  starting transfers between devices  41.6 us (25%)
  Pallas kernels  40.2 us (24%)
  local copies, waits for them, and re-layouts  10.7 us (6%)
  other arithmetic  2.81 us (2%)
    ppermute x27, waiting for transfers between devices, across(): return lax.ppermute(value, axis, [(i, i ^ k) for i in range(count)])  51.6 us
    ppermute x27, starting transfers between devices, across(): return lax.ppermute(value, axis, [(i, i ^ k) for i in range(count)])  30.9 us
    pallas_call x1, Pallas kernels, shards(): pl.pallas_call(functools.partial(scan_kernel, parts=tuple(parts), planes=...  12.8 us
    pallas_call x2, Pallas kernels, attend(): pl.pallas_call(functools.partial(attention_kernel, planes=B, cores=T, slo...  11 us
    ppermute x3, waiting for transfers between devices, ring(): moving = lax.ppermute(moving, axis, pairs)  9.33 us
    unnamed x64, local copies, waits for them, and re-layouts  5.98 us
    ppermute x3, starting transfers between devices, ring(): moving = lax.ppermute(moving, axis, pairs)  5.48 us
    pallas_call x1, Pallas kernels, shards(): pl.pallas_call(functools.partial(gate_kernel, parts=tuple(parts), planes=...  5.15 us
  transfers between devices with their start and end apart: 32, of which 8 were waited for; matrix products, arithmetic and copies ran while one was open for 4% of the time, Pallas kernels for 20%

profile of v2, /device:TPU:8, one launch (start us, length us, event | category | flops | bytes accessed | tf_op | source)
XLA Modules:
  0.0 165.0 jit_solution(4976956650099999833)
XLA Ops:
  0.8 0.6 pad_add_fusion.where_ref
  1.4 1.3 fusion
  2.7 3.8 %prologue.1 = (bf16[128,2176]{1,0:T(8,128)(2,1)}, bf16[128,384]{1,0:T(8,128)(2,1)}, bf16[8,2048]{1,0:T(8,128)(2,1)}) custom-call(s32[3]{0:T(128)} %pad_add_fusion.where_ref, bf16[128,2048]{1,0:T(8,128)(2,1)} %tokens_ref.1, f32[1,2048]{1,0:T(1,128)} %bitcast.43, bf16[2048,256]{1,0:T(8,128)(2,1)} %proj_ref.1, f32[1,256]{1,0:T(1,128)} %bitcast.45, ...), custom_call_target="tpu_custom_call" | custom-call | flops 536870912 | bytes 536870 | tf_op jit(solution)/shard_map/prologue/pallas_call | solution.py:628
  6.5 3.0 %collective-permute-start.5 = (bf16[128,384]{1,0:T(8,128)(2,1)}, bf16[128,384]{1,0:T(8,128)(2,1)S(1)}, u32[]{:S(2)}, u32[]{:S(2)}) collective-permute-start(bf16[128,384]{1,0:T(8,128)(2,1)} %get-tuple-element.33), channel_id=1, source_target_pairs={{0,16},{8,24},{16,0},{24,8},{1,17},{9,25},{17,1},{25,9},{2,18},{10... | collective-permute-start | bytes 294920 | tf_op jit(solution)/shard_map/ppermute | solution.py:72
  9.9 1.0 constant_dynamic-slice_fusion.15
  11.1 1.6 collective-permute-start.1
  12.7 1.6 collective-permute-start.7
  14.2 0.9 constant_dynamic-update-slice_fusion.3
  15.2 3.4 %collective-permute-done.7 = bf16[8,2048]{1,0:T(8,128)(2,1)S(1)} collective-permute-done((bf16[8,2048]{1,0:T(8,128)(2,1)}, bf16[8,2048]{1,0:T(8,128)(2,1)S(1)}, u32[]{:S(2)}, u32[]{:S(2)}) %collective-permute-start.7) | collective-permute-done | bytes 32800 | tf_op jit(solution)/shard_map/ppermute | solution.py:663
  18.6 1.5 collective-permute-start.2
  20.2 1.5 collective-permute-start.3
  21.8 6.8 %collective-permute-done.2 = bf16[128,768]{1,0:T(8,128)(2,1)S(1)} collective-permute-done((bf16[128,768]{1,0:T(8,128)(2,1)S(1)}, bf16[128,768]{1,0:T(8,128)(2,1)S(1)}, u32[]{:S(2)}, u32[]{:S(2)}) %collective-permute-start.2) | collective-permute-done | bytes 196640 | tf_op jit(solution)/shard_map/ppermute | solution.py:72
  28.7 0.7 copy-done.14
  29.4 0.8 pad_maximum_fusion.refs_8_
  30.2 1.5 collective-permute-start.9
  31.7 1.6 collective-permute-start.11
  34.4 8.6 %collective-permute-done.9.refs_2_.refs_14_ = bf16[560,384]{1,0:T(8,128)(2,1)S(1)} collective-permute-done((bf16[560,384]{1,0:T(8,128)(2,1)S(1)}, bf16[560,384]{1,0:T(8,128)(2,1)S(1)}, u32[]{:S(2)}, u32[]{:S(2)}) %collective-permute-start.9) | collective-permute-done | bytes 430112 | tf_op jit(solution)/shard_map/ppermute | solution.py:72
  43.0 2.4 %collective-permute-start.20 = (bf16[128,2176]{1,0:T(8,128)(2,1)S(1)}, bf16[128,2176]{1,0:T(8,128)(2,1)S(1)}, u32[]{:S(2)}, u32[]{:S(2)}) collective-permute-start(bf16[128,2176]{1,0:T(8,128)(2,1)S(1)} %copy-done), channel_id=1, source_target_pairs={{0,6},{2,4},{4,2},{6,0},{1,7},{3,5},{5,3},{7,1},{8,14},{10,12},{12... | collective-permute-start | bytes 1671176 | tf_op jit(solution)/shard_map/ppermute | solution.py:72
  45.5 0.6 collective-permute-start.13
  46.1 0.6 collective-permute-start.14
  46.7 25.8 %collective-permute-done.13 = bf16[280,384]{1,0:T(8,128)(2,1)S(1)} collective-permute-done((bf16[280,384]{1,0:T(8,128)(2,1)S(1)}, bf16[280,384]{1,0:T(8,128)(2,1)S(1)}, u32[]{:S(2)}, u32[]{:S(2)}) %collective-permute-start.13) | collective-permute-done | bytes 215072 | tf_op jit(solution)/shard_map/ppermute | solution.py:72
  72.5 2.4 %collective-permute-start.22 = (bf16[512,512]{1,0:T(8,128)(2,1)}, bf16[512,512]{1,0:T(8,128)(2,1)}, u32[]{:S(2)}, u32[]{:S(2)}) collective-permute-start(bf16[512,512]{1,0:T(8,128)(2,1)} %pad_maximum_fusion.refs_8_), channel_id=1, source_target_pairs={{0,8},{8,16},{16,24},{24,0},{1,9},{9,17},{17,25},{25,1},{2,10},{10... | collective-permute-start | bytes 1572872 | tf_op jit(solution)/shard_map/ppermute | solution.py:84
  76.2 0.6 collective-permute-done.8.refs_1_.refs_13_
  76.9 9.3 %collective-permute-done.22.refs_9_ = bf16[512,512]{1,0:T(8,128)(2,1)} collective-permute-done((bf16[512,512]{1,0:T(8,128)(2,1)}, bf16[512,512]{1,0:T(8,128)(2,1)}, u32[]{:S(2)}, u32[]{:S(2)}) %collective-permute-start.22) | collective-permute-done | bytes 524320 | tf_op jit(solution)/shard_map/ppermute | solution.py:84
  86.3 0.6 collective-permute-start.21
  86.8 2.1 %collective-permute-start.24 = (bf16[512,512]{1,0:T(8,128)(2,1)}, bf16[512,512]{1,0:T(8,128)(2,1)}, u32[]{:S(2)}, u32[]{:S(2)}) collective-permute-start(bf16[512,512]{1,0:T(8,128)(2,1)} %pad_maximum_fusion.refs_8_), channel_id=1, source_target_pairs={{0,24},{8,0},{16,8},{24,16},{1,25},{9,1},{17,9},{25,17},{2,26},{10... | collective-permute-start | bytes 1572872 | tf_op jit(solution)/shard_map/ppermute | solution.py:84
  89.0 0.8 copy-done.28
  89.7 1.0 collective-permute-start.23
  90.7 1.8 %copy.22 = bf16[256,512]{0,1:T(8,128)(2,1)} copy(bf16[256,512]{1,0:T(8,128)(2,1)} %param.27) | data formatting | bytes 524288 | tf_op args[7]
  92.5 0.8 slice.42
  93.4 0.8 slice.43
  94.2 0.8 slice.44
  95.1 4.2 %query.1 = (bf16[256,512]{1,0:T(8,128)(2,1)}, bf16[256,256]{1,0:T(8,128)(2,1)}) custom-call(s32[3]{0:T(128)} %pad_add_fusion.where_ref, bf16[128,2176]{1,0:T(8,128)(2,1)} %get-tuple-element.28.refs_0_, bf16[128,2176]{1,0:T(8,128)(2,1)} %copy-done.1, bf16[2048,768]{1,0:T(8,128)(2,1)} %refs_2_.1, f32[256,128]{1,0:T(8,128)} %get-tuple-element.74.cos_ref.refs_3_, ...), custom_call_target="tpu_custom_call" | custom-call | flops 1073741824 | bytes 1073741 | tf_op jit(solution)/shard_map/query/pallas_call | solution.py:698
  99.3 8.6 %attention.2 = (f32[4,1,256]{2,1,0:T(1,128)}, f32[4,1,256]{2,1,0:T(1,128)}, f32[4,128,256]{2,1,0:T(8,128)}) custom-call(s32[3]{0:T(128)} %pad_add_fusion.where_ref, bf16[256,512]{1,0:T(8,128)(2,1)} %get-tuple-element.29.plain_ref, bf16[256,256]{1,0:T(8,128)(2,1)} %get-tuple-element.30.turned_ref, bf16[256,512]{1,0:T(8,128)(2,1)} %ku_ref.3, ...), custom_call_target="tpu_custom_call" | custom-call | flops 2684354560 | bytes 2684354 | tf_op jit(solution)/shard_map/attention/pallas_call | solution.py:716
  108.1 8.3 %collective-permute-start.29 = (bf16[512,256]{1,0:T(8,128)(2,1)S(1)}, bf16[512,256]{1,0:T(8,128)(2,1)S(1)}, u32[]{:S(2)}, u32[]{:S(2)}) collective-permute-start(bf16[512,256]{1,0:T(8,128)(2,1)S(1)} %pad_maximum_fusion.1.refs_8_), channel_id=1, source_target_pairs={{0,16},{8,24},{16,0},{24,8},{1,17},{9,25},{17,1},{25,9},{2,18},{10... | collective-permute-start | bytes 786440 | tf_op jit(solution)/shard_map/ppermute | solution.py:72
  116.3 0.6 collective-permute-start.30
  117.2 12.8 %state_scan.1 = (f32[1024,256]{1,0:T(8,128)}, bf16[1024,128]{1,0:T(8,128)(2,1)}, f32[1024,128]{1,0:T(8,128)}, bf16[144,256]{1,0:T(8,128)(2,1)}) custom-call(s32[3]{0:T(128)} %pad_add_fusion.where_ref, bf16[128,2176]{1,0:T(8,128)(2,1)} %get-tuple-element.28.refs_0_, bf16[128,2176]{1,0:T(8,128)(2,1)} %copy-done.1, bf16[128,2176]{1,0:T(8,128)(2,1)} %copy-done.3, ...), custom_call_target="tpu_custom_call" | custom-call | flops 4294967296 | bytes 4294967 | tf_op jit(solution)/shard_map/state_scan/pallas_call | solution.py:745
  129.9 2.0 %collective-permute-start.25 = (bf16[144,256]{1,0:T(8,128)(2,1)}, bf16[144,256]{1,0:T(8,128)(2,1)S(1)}, u32[]{:S(2)}, u32[]{:S(2)}) collective-permute-start(bf16[144,256]{1,0:T(8,128)(2,1)} %get-tuple-element.44.refs_0_), channel_id=1, source_target_pairs={{0,8},{8,0},{16,24},{24,16},{1,9},{9,1},{17,25},{25,17},{2,10},{10... | collective-permute-start | bytes 221192 | tf_op jit(solution)/shard_map/ppermute | solution.py:72
  131.9 1.8 %collective-permute-start.26 = (bf16[144,256]{1,0:T(8,128)(2,1)}, bf16[144,256]{1,0:T(8,128)(2,1)S(1)}, u32[]{:S(2)}, u32[]{:S(2)}) collective-permute-start(bf16[144,256]{1,0:T(8,128)(2,1)} %get-tuple-element.44.refs_0_), channel_id=1, source_target_pairs={{0,16},{8,24},{16,0},{24,8},{1,17},{9,25},{17,1},{25,9},{2,18},{10... | collective-permute-start | bytes 221192 | tf_op jit(solution)/shard_map/ppermute | solution.py:72
  134.3 9.7 %collective-permute-done.30.refs_11_ = bf16[512,256]{1,0:T(8,128)(2,1)S(1)} collective-permute-done((bf16[512,256]{1,0:T(8,128)(2,1)S(1)}, bf16[512,256]{1,0:T(8,128)(2,1)S(1)}, u32[]{:S(2)}, u32[]{:S(2)}) %collective-permute-start.30) | collective-permute-done | bytes 262176 | tf_op jit(solution)/shard_map/ppermute | solution.py:72
  144.0 0.7 copy-done.10
  144.7 5.1 %gate.1.refs_6_ = bf16[1024,256]{1,0:T(8,128)(2,1)} custom-call(s32[3]{0:T(128)} %pad_add_fusion.where_ref, bf16[128,2176]{1,0:T(8,128)(2,1)} %get-tuple-element.28.refs_0_, bf16[128,2176]{1,0:T(8,128)(2,1)} %copy-done.1, bf16[128,2176]{1,0:T(8,128)(2,1)} %copy-done.3, bf16[128,2176]{1,0:T(8,128)(2,1)} %copy-done.6, bf16[128,2176]{1,0:T(8,128)(2,1)} %copy-done.4, ...), custom_call_target="tpu_custom_call" | custom-call | flops 1073741824 | bytes 1073741 | tf_op jit(solution)/shard_map/gate/pallas_call | solution.py:795
  149.9 0.6 copy-done.20
  150.6 3.3 %finish.1 = bf16[1024,256]{1,0:T(8,128)(2,1)} custom-call(s32[3]{0:T(128)} %pad_add_fusion.where_ref, bf16[144,256]{1,0:T(8,128)(2,1)} %get-tuple-element.44.refs_0_, bf16[144,256]{1,0:T(8,128)(2,1)} %copy-done.20, bf16[144,256]{1,0:T(8,128)(2,1)} %copy-done.21, bf16[144,256]{1,0:T(8,128)(2,1)} %copy-done.22, f32[1024,256]{1,0:T(8,128)} %get-tuple-element.45.refs_4_, ...), custom_call_target="tpu_custom_call" | custom-call | tf_op jit(solution)/shard_map/finish/pallas_call | solution.py:813
  153.9 3.6 %all-to-all-start = ((bf16[4,256,256]{2,1,0:T(8,128)(2,1)}), bf16[4,256,256]{2,1,0:T(8,128)(2,1)S(1)}, u32[]{:S(2)}, u32[]{:S(2)}) async-start(bf16[4,256,256]{2,1,0:T(8,128)(2,1)} %bitcast.36), calls=%async_computation | async-start | bytes 1048576 | tf_op jit(solution)/shard_map/all_to_all | solution.py:837
  157.5 2.4 %attention.3 = bf16[256,512]{1,0:T(8,128)(2,1)} custom-call(s32[3]{0:T(128)} %pad_add_fusion.where_ref, bf16[256,512]{1,0:T(8,128)(2,1)} %get-tuple-element.29.plain_ref, bf16[256,256]{1,0:T(8,128)(2,1)} %get-tuple-element.30.turned_ref, bf16[256,512]{1,0:T(8,128)(2,1)} %ku_ref.3, bf16[512,256]{1,0:T(8,128)(2,1)} %bitcast.40, bf16[560,384]{1,0:T(8,128)(2,1)} %copy-done.23, ...), custom_call_target="tpu_custom_call" | custom-call | flops 1610612736 | bytes 1610612 | tf_op jit(solution)/shard_map/attention/pallas_call | solution.py:716
  159.9 4.2 %all-to-all-done = bf16[4,256,256]{2,1,0:T(8,128)(2,1)S(1)} async-done(((bf16[4,256,256]{2,1,0:T(8,128)(2,1)}), bf16[4,256,256]{2,1,0:T(8,128)(2,1)S(1)}, u32[]{:S(2)}, u32[]{:S(2)}) %all-to-all-start) | async-done | bytes 524320 | tf_op jit(solution)/shard_map/all_to_all | solution.py:837
  164.1 0.9 copy.24
  (117 shorter events, 4.4 us)
Async XLA Ops:
  0.6 10.3 %copy-start.11 = (bf16[128,1024]{1,0:T(8,128)(2,1)S(1)}, bf16[128,1024]{1,0:T(8,128)(2,1)}, u32[]{:S(2)}) copy-start(bf16[128,1024]{1,0:T(8,128)(2,1)} %param.29) | copy-start | bytes 786436
  0.6 10.3 %copy-start.16 = (bf16[128,512]{1,0:T(8,128)(2,1)S(1)}, bf16[128,512]{1,0:T(8,128)(2,1)}, u32[]{:S(2)}) copy-start(bf16[128,512]{1,0:T(8,128)(2,1)} %param.30) | copy-start | bytes 393220
  0.7 10.3 %copy-start.15 = (bf16[128,512]{1,0:T(8,128)(2,1)S(1)}, bf16[128,512]{1,0:T(8,128)(2,1)}, u32[]{:S(2)}) copy-start(bf16[128,512]{1,0:T(8,128)(2,1)} %param.31) | copy-start | bytes 393220
  0.7 14.5 %copy-start.24 = (f32[256,16]{0,1:T(8,128)S(1)}, f32[256,16]{0,1:T(8,128)}, u32[]{:S(2)}) copy-start(f32[256,16]{0,1:T(8,128)} %param.37) | copy-start | bytes 49156
  6.5 25.3 %copy-start = (bf16[128,2176]{1,0:T(8,128)(2,1)S(1)}, bf16[128,2176]{1,0:T(8,128)(2,1)}, u32[]{:S(2)}) copy-start(bf16[128,2176]{1,0:T(8,128)(2,1)} %get-tuple-element.28.refs_0_) | copy-start | bytes 1671172
  6.5 13.7 %collective-permute-start.4 = (bf16[128,384]{1,0:T(8,128)(2,1)}, bf16[128,384]{1,0:T(8,128)(2,1)S(1)}, u32[]{:S(2)}, u32[]{:S(2)}) collective-permute-start(bf16[128,384]{1,0:T(8,128)(2,1)} %get-tuple-element.33), channel_id=1, source_target_pairs={{0,8},{8,0},{16,24},{24,16},{1,9},{9,1},{17,25},{25,17},{2,10},{10... | collective-permute-start | bytes 294920 | tf_op jit(solution)/shard_map/ppermute | solution.py:72
  6.5 15.2 %collective-permute-start.5 = (bf16[128,384]{1,0:T(8,128)(2,1)}, bf16[128,384]{1,0:T(8,128)(2,1)S(1)}, u32[]{:S(2)}, u32[]{:S(2)}) collective-permute-start(bf16[128,384]{1,0:T(8,128)(2,1)} %get-tuple-element.33), channel_id=1, source_target_pairs={{0,16},{8,24},{16,0},{24,8},{1,17},{9,25},{17,1},{25,9},{2,18},{10... | collective-permute-start | bytes 294920 | tf_op jit(solution)/shard_map/ppermute | solution.py:72
  9.5 12.2 %collective-permute-start.6 = (bf16[128,384]{1,0:T(8,128)(2,1)}, bf16[128,384]{1,0:T(8,128)(2,1)S(1)}, u32[]{:S(2)}, u32[]{:S(2)}) collective-permute-start(bf16[128,384]{1,0:T(8,128)(2,1)} %get-tuple-element.33), channel_id=1, source_target_pairs={{0,24},{8,16},{16,8},{24,0},{1,25},{9,17},{17,9},{25,1},{2,26},{10... | collective-permute-start | bytes 294920 | tf_op jit(solution)/shard_map/ppermute | solution.py:72
  11.1 10.7 %collective-permute-start.1 = (bf16[128,768]{1,0:T(8,128)(2,1)S(1)}, bf16[128,768]{1,0:T(8,128)(2,1)S(1)}, u32[]{:S(2)}, u32[]{:S(2)}) collective-permute-start(bf16[128,768]{1,0:T(8,128)(2,1)S(1)} %pad_maximum_fusion.2), channel_id=1, source_target_pairs={{0,2},{2,0},{4,6},{6,4},{1,3},{3,1},{5,7},{7,5},{8,10},{10,8},{12,... | collective-permute-start | bytes 589832 | tf_op jit(solution)/shard_map/ppermute | solution.py:72
  12.7 5.9 %collective-permute-start.7 = (bf16[8,2048]{1,0:T(8,128)(2,1)}, bf16[8,2048]{1,0:T(8,128)(2,1)S(1)}, u32[]{:S(2)}, u32[]{:S(2)}) collective-permute-start(bf16[8,2048]{1,0:T(8,128)(2,1)} %get-tuple-element.34), channel_id=1, source_target_pairs={{0,8},{8,16},{16,24},{24,0},{1,9},{9,17},{17,25},{25,1},{2,10},{10... | collective-permute-start | bytes 98312 | tf_op jit(solution)/shard_map/ppermute | solution.py:663
  18.6 10.0 %collective-permute-start.2 = (bf16[128,768]{1,0:T(8,128)(2,1)S(1)}, bf16[128,768]{1,0:T(8,128)(2,1)S(1)}, u32[]{:S(2)}, u32[]{:S(2)}) collective-permute-start(bf16[128,768]{1,0:T(8,128)(2,1)S(1)} %pad_maximum_fusion.3), channel_id=1, source_target_pairs={{0,4},{2,6},{4,0},{6,2},{1,5},{3,7},{5,1},{7,3},{8,12},{10,14},{12... | collective-permute-start | bytes 589832 | tf_op jit(solution)/shard_map/ppermute | solution.py:72
  20.2 8.5 %collective-permute-start.3 = (bf16[128,768]{1,0:T(8,128)(2,1)S(1)}, bf16[128,768]{1,0:T(8,128)(2,1)S(1)}, u32[]{:S(2)}, u32[]{:S(2)}) collective-permute-start(bf16[128,768]{1,0:T(8,128)(2,1)S(1)} %pad_maximum_fusion.4), channel_id=1, source_target_pairs={{0,6},{2,4},{4,2},{6,0},{1,7},{3,5},{5,3},{7,1},{8,14},{10,12},{12... | collective-permute-start | bytes 589832 | tf_op jit(solution)/shard_map/ppermute | solution.py:72
  21.8 55.1 %copy-start.23 = (bf16[560,384]{1,0:T(8,128)(2,1)}, bf16[560,384]{1,0:T(8,128)(2,1)S(1)}, u32[]{:S(2)}) copy-start(bf16[560,384]{1,0:T(8,128)(2,1)S(1)} %maximum_dynamic-update-slice_fusion.refs_0_.refs_12_) | copy-start | bytes 1290244
  21.8 12.5 %copy-start.12 = (bf16[128,768]{1,0:T(8,128)(2,1)}, bf16[128,768]{1,0:T(8,128)(2,1)S(1)}, u32[]{:S(2)}) copy-start(bf16[128,768]{1,0:T(8,128)(2,1)S(1)} %collective-permute-done.1) | copy-start | bytes 589828
  30.2 12.8 %collective-permute-start.9 = (bf16[560,384]{1,0:T(8,128)(2,1)S(1)}, bf16[560,384]{1,0:T(8,128)(2,1)S(1)}, u32[]{:S(2)}, u32[]{:S(2)}) collective-permute-start(bf16[560,384]{1,0:T(8,128)(2,1)S(1)} %maximum_dynamic-update-slice_fusion.refs_0_.refs_12_), channel_id=1, source_target_pairs={{0,2},{2,0},{4,6},{6,4},{1,3},{3,1},{5,7},{7,5},{8,10},{10,8},{12,... | collective-permute-start | bytes 1290248 | tf_op jit(solution)/shard_map/ppermute | solution.py:72
  31.7 14.4 %collective-permute-start = (bf16[128,2176]{1,0:T(8,128)(2,1)S(1)}, bf16[128,2176]{1,0:T(8,128)(2,1)S(1)}, u32[]{:S(2)}, u32[]{:S(2)}) collective-permute-start(bf16[128,2176]{1,0:T(8,128)(2,1)S(1)} %copy-done), channel_id=1, source_target_pairs={{0,1},{1,0},{2,3},{3,2},{4,5},{5,4},{6,7},{7,6},{8,9},{9,8},{10,11... | collective-permute-start | bytes 1671176 | tf_op jit(solution)/shard_map/ppermute | solution.py:72
  31.7 13.8 %collective-permute-start.11 = (bf16[560,384]{1,0:T(8,128)(2,1)S(1)}, bf16[560,384]{1,0:T(8,128)(2,1)S(1)}, u32[]{:S(2)}, u32[]{:S(2)}) collective-permute-start(bf16[560,384]{1,0:T(8,128)(2,1)S(1)} %maximum_dynamic-update-slice_fusion.refs_0_.refs_12_), channel_id=1, source_target_pairs={{0,4},{2,6},{4,0},{6,2},{1,5},{3,7},{5,1},{7,3},{8,12},{10,14},{12... | collective-permute-start | bytes 1290248 | tf_op jit(solution)/shard_map/ppermute | solution.py:72
  33.3 41.6 %collective-permute-start.16 = (bf16[128,2176]{1,0:T(8,128)(2,1)S(1)}, bf16[128,2176]{1,0:T(8,128)(2,1)S(1)}, u32[]{:S(2)}, u32[]{:S(2)}) collective-permute-start(bf16[128,2176]{1,0:T(8,128)(2,1)S(1)} %copy-done), channel_id=1, source_target_pairs={{0,2},{2,0},{4,6},{6,4},{1,3},{3,1},{5,7},{7,5},{8,10},{10,8},{12,... | collective-permute-start | bytes 1671176 | tf_op jit(solution)/shard_map/ppermute | solution.py:72
  33.8 41.2 %collective-permute-start.18 = (bf16[128,2176]{1,0:T(8,128)(2,1)S(1)}, bf16[128,2176]{1,0:T(8,128)(2,1)S(1)}, u32[]{:S(2)}, u32[]{:S(2)}) collective-permute-start(bf16[128,2176]{1,0:T(8,128)(2,1)S(1)} %copy-done), channel_id=1, source_target_pairs={{0,4},{2,6},{4,0},{6,2},{1,5},{3,7},{5,1},{7,3},{8,12},{10,14},{12... | collective-permute-start | bytes 1671176 | tf_op jit(solution)/shard_map/ppermute | solution.py:72
  43.0 43.2 %copy-start.17 = (bf16[560,384]{1,0:T(8,128)(2,1)}, bf16[560,384]{1,0:T(8,128)(2,1)S(1)}, u32[]{:S(2)}) copy-start(bf16[560,384]{1,0:T(8,128)(2,1)S(1)} %collective-permute-done.9.refs_2_.refs_14_) | copy-start | bytes 1290244
  43.0 32.7 %collective-permute-start.20 = (bf16[128,2176]{1,0:T(8,128)(2,1)S(1)}, bf16[128,2176]{1,0:T(8,128)(2,1)S(1)}, u32[]{:S(2)}, u32[]{:S(2)}) collective-permute-start(bf16[128,2176]{1,0:T(8,128)(2,1)S(1)} %copy-done), channel_id=1, source_target_pairs={{0,6},{2,4},{4,2},{6,0},{1,7},{3,5},{5,3},{7,1},{8,14},{10,12},{12... | collective-permute-start | bytes 1671176 | tf_op jit(solution)/shard_map/ppermute | solution.py:72
  45.5 40.8 %copy-start.18 = (bf16[560,384]{1,0:T(8,128)(2,1)}, bf16[560,384]{1,0:T(8,128)(2,1)S(1)}, u32[]{:S(2)}) copy-start(bf16[560,384]{1,0:T(8,128)(2,1)S(1)} %collective-permute-done.11.refs_4_.refs_16_) | copy-start | bytes 1290244
  45.5 27.0 %collective-permute-start.13 = (bf16[280,384]{1,0:T(8,128)(2,1)S(1)}, bf16[280,384]{1,0:T(8,128)(2,1)S(1)}, u32[]{:S(2)}, u32[]{:S(2)}) collective-permute-start(bf16[280,384]{1,0:T(8,128)(2,1)S(1)} %slice.40), channel_id=1, source_target_pairs={{0,4},{2,6},{4,0},{6,2},{1,5},{3,7},{5,1},{7,3},{8,12},{10,14},{12... | collective-permute-start | bytes 645128 | tf_op jit(solution)/shard_map/ppermute | solution.py:72
  46.1 49.0 %copy-start.1 = (bf16[128,2176]{1,0:T(8,128)(2,1)}, bf16[128,2176]{1,0:T(8,128)(2,1)S(1)}, u32[]{:S(2)}) copy-start(bf16[128,2176]{1,0:T(8,128)(2,1)S(1)} %collective-permute-done.refs_1_) | copy-start | bytes 1671172
  46.1 29.4 %collective-permute-start.14 = (bf16[280,384]{1,0:T(8,128)(2,1)S(1)}, bf16[280,384]{1,0:T(8,128)(2,1)S(1)}, u32[]{:S(2)}, u32[]{:S(2)}) collective-permute-start(bf16[280,384]{1,0:T(8,128)(2,1)S(1)} %slice.41), channel_id=1, source_target_pairs={{0,2},{2,0},{4,6},{6,4},{1,3},{3,1},{5,7},{7,5},{8,10},{10,8},{12,... | collective-permute-start | bytes 645128 | tf_op jit(solution)/shard_map/ppermute | solution.py:72
  72.5 13.7 %collective-permute-start.22 = (bf16[512,512]{1,0:T(8,128)(2,1)}, bf16[512,512]{1,0:T(8,128)(2,1)}, u32[]{:S(2)}, u32[]{:S(2)}) collective-permute-start(bf16[512,512]{1,0:T(8,128)(2,1)} %pad_maximum_fusion.refs_8_), channel_id=1, source_target_pairs={{0,8},{8,16},{16,24},{24,0},{1,9},{9,17},{17,25},{25,1},{2,10},{10... | collective-permute-start | bytes 1572872 | tf_op jit(solution)/shard_map/ppermute | solution.py:84
  74.9 24.4 %copy-start.3 = (bf16[128,2176]{1,0:T(8,128)(2,1)}, bf16[128,2176]{1,0:T(8,128)(2,1)S(1)}, u32[]{:S(2)}) copy-start(bf16[128,2176]{1,0:T(8,128)(2,1)S(1)} %collective-permute-done.16.refs_2_) | copy-start | bytes 1671172
  74.9 1.8 %collective-permute-start.8 = (bf16[560,384]{1,0:T(8,128)(2,1)S(1)}, bf16[560,384]{1,0:T(8,128)(2,1)S(1)}, u32[]{:S(2)}, u32[]{:S(2)}) collective-permute-start(bf16[560,384]{1,0:T(8,128)(2,1)S(1)} %maximum_dynamic-update-slice_fusion.refs_0_.refs_12_), channel_id=1, source_target_pairs={{0,1},{1,0},{2,3},{3,2},{4,5},{5,4},{6,7},{7,6},{8,9},{9,8},{10,11... | collective-permute-start | bytes 1290248 | tf_op jit(solution)/shard_map/ppermute | solution.py:72
  75.0 24.3 %copy-start.4 = (bf16[128,2176]{1,0:T(8,128)(2,1)}, bf16[128,2176]{1,0:T(8,128)(2,1)S(1)}, u32[]{:S(2)}) copy-start(bf16[128,2176]{1,0:T(8,128)(2,1)S(1)} %collective-permute-done.18.refs_4_) | copy-start | bytes 1671172
  75.0 11.2 %collective-permute-start.10 = (bf16[560,384]{1,0:T(8,128)(2,1)S(1)}, bf16[560,384]{1,0:T(8,128)(2,1)S(1)}, u32[]{:S(2)}, u32[]{:S(2)}) collective-permute-start(bf16[560,384]{1,0:T(8,128)(2,1)S(1)} %collective-permute-done.9.refs_2_.refs_14_), channel_id=1, source_target_pairs={{0,1},{1,0},{2,3},{3,2},{4,5},{5,4},{6,7},{7,6},{8,9},{9,8},{10,11... | collective-permute-start | bytes 1290248 | tf_op jit(solution)/shard_map/ppermute | solution.py:72
  75.5 11.3 %collective-permute-start.12 = (bf16[560,384]{1,0:T(8,128)(2,1)S(1)}, bf16[560,384]{1,0:T(8,128)(2,1)S(1)}, u32[]{:S(2)}, u32[]{:S(2)}) collective-permute-start(bf16[560,384]{1,0:T(8,128)(2,1)S(1)} %collective-permute-done.11.refs_4_.refs_16_), channel_id=1, source_target_pairs={{0,1},{1,0},{2,3},{3,2},{4,5},{5,4},{6,7},{7,6},{8,9},{9,8},{10,11... | collective-permute-start | bytes 1290248 | tf_op jit(solution)/shard_map/ppermute | solution.py:72
  75.7 11.2 %copy-start.19 = (bf16[560,384]{1,0:T(8,128)(2,1)}, bf16[560,384]{1,0:T(8,128)(2,1)S(1)}, u32[]{:S(2)}) copy-start(bf16[560,384]{1,0:T(8,128)(2,1)S(1)} %constant_dynamic-update-slice_fusion.4.refs_6_.refs_18_) | copy-start | bytes 1290244
  75.7 32.3 %copy-start.5 = (bf16[128,2176]{1,0:T(8,128)(2,1)}, bf16[128,2176]{1,0:T(8,128)(2,1)S(1)}, u32[]{:S(2)}) copy-start(bf16[128,2176]{1,0:T(8,128)(2,1)S(1)} %collective-permute-done.20.refs_6_) | copy-start | bytes 1671172
  75.7 13.2 %collective-permute-start.15 = (bf16[560,384]{1,0:T(8,128)(2,1)S(1)}, bf16[560,384]{1,0:T(8,128)(2,1)S(1)}, u32[]{:S(2)}, u32[]{:S(2)}) collective-permute-start(bf16[560,384]{1,0:T(8,128)(2,1)S(1)} %constant_dynamic-update-slice_fusion.4.refs_6_.refs_18_), channel_id=1, source_target_pairs={{0,1},{1,0},{2,3},{3,2},{4,5},{5,4},{6,7},{7,6},{8,9},{9,8},{10,11... | collective-permute-start | bytes 1290248 | tf_op jit(solution)/shard_map/ppermute | solution.py:72
  76.8 12.2 %copy-start.25 = (bf16[560,384]{1,0:T(8,128)(2,1)}, bf16[560,384]{1,0:T(8,128)(2,1)S(1)}, u32[]{:S(2)}) copy-start(bf16[560,384]{1,0:T(8,128)(2,1)S(1)} %collective-permute-done.8.refs_1_.refs_13_) | copy-start | bytes 1290244
  76.8 31.3 %collective-permute-start.17 = (bf16[128,2176]{1,0:T(8,128)(2,1)S(1)}, bf16[128,2176]{1,0:T(8,128)(2,1)S(1)}, u32[]{:S(2)}, u32[]{:S(2)}) collective-permute-start(bf16[128,2176]{1,0:T(8,128)(2,1)S(1)} %collective-permute-done.16.refs_2_), channel_id=1, source_target_pairs={{0,1},{1,0},{2,3},{3,2},{4,5},{5,4},{6,7},{7,6},{8,9},{9,8},{10,11... | collective-permute-start | bytes 1671176 | tf_op jit(solution)/shard_map/ppermute | solution.py:72
  86.2 30.1 %collective-permute-start.19 = (bf16[128,2176]{1,0:T(8,128)(2,1)S(1)}, bf16[128,2176]{1,0:T(8,128)(2,1)S(1)}, u32[]{:S(2)}, u32[]{:S(2)}) collective-permute-start(bf16[128,2176]{1,0:T(8,128)(2,1)S(1)} %collective-permute-done.18.refs_4_), channel_id=1, source_target_pairs={{0,1},{1,0},{2,3},{3,2},{4,5},{5,4},{6,7},{7,6},{8,9},{9,8},{10,11... | collective-permute-start | bytes 1671176 | tf_op jit(solution)/shard_map/ppermute | solution.py:72
  86.3 30.6 %collective-permute-start.21 = (bf16[128,2176]{1,0:T(8,128)(2,1)S(1)}, bf16[128,2176]{1,0:T(8,128)(2,1)}, u32[]{:S(2)}, u32[]{:S(2)}) collective-permute-start(bf16[128,2176]{1,0:T(8,128)(2,1)S(1)} %collective-permute-done.20.refs_6_), channel_id=1, source_target_pairs={{0,1},{1,0},{2,3},{3,2},{4,5},{5,4},{6,7},{7,6},{8,9},{9,8},{10,11... | collective-permute-start | bytes 1671176 | tf_op jit(solution)/shard_map/ppermute | solution.py:72
  86.8 21.1 %collective-permute-start.24 = (bf16[512,512]{1,0:T(8,128)(2,1)}, bf16[512,512]{1,0:T(8,128)(2,1)}, u32[]{:S(2)}, u32[]{:S(2)}) collective-permute-start(bf16[512,512]{1,0:T(8,128)(2,1)} %pad_maximum_fusion.refs_8_), channel_id=1, source_target_pairs={{0,24},{8,0},{16,8},{24,16},{1,25},{9,1},{17,9},{25,17},{2,26},{10... | collective-permute-start | bytes 1572872 | tf_op jit(solution)/shard_map/ppermute | solution.py:84
  89.7 27.2 %collective-permute-start.23 = (bf16[512,512]{1,0:T(8,128)(2,1)}, bf16[512,512]{1,0:T(8,128)(2,1)}, u32[]{:S(2)}, u32[]{:S(2)}) collective-permute-start(bf16[512,512]{1,0:T(8,128)(2,1)} %collective-permute-done.22.refs_9_), channel_id=1, source_target_pairs={{0,8},{8,16},{16,24},{24,0},{1,9},{9,17},{17,25},{25,1},{2,10},{10... | collective-permute-start | bytes 1572872 | tf_op jit(solution)/shard_map/ppermute | solution.py:84
  95.1 21.2 %copy-start.2 = (bf16[512,256]{1,0:T(8,128)(2,1)}, bf16[512,256]{1,0:T(8,128)(2,1)S(1)}, u32[]{:S(2)}) copy-start(bf16[512,256]{1,0:T(8,128)(2,1)S(1)} %pad_maximum_fusion.1.refs_8_) | copy-start | bytes 786436
  108.0 25.8 %collective-permute-start.28 = (bf16[512,256]{1,0:T(8,128)(2,1)S(1)}, bf16[512,256]{1,0:T(8,128)(2,1)S(1)}, u32[]{:S(2)}, u32[]{:S(2)}) collective-permute-start(bf16[512,256]{1,0:T(8,128)(2,1)S(1)} %pad_maximum_fusion.1.refs_8_), channel_id=1, source_target_pairs={{0,8},{8,0},{16,24},{24,16},{1,9},{9,1},{17,25},{25,17},{2,10},{10... | collective-permute-start | bytes 786440 | tf_op jit(solution)/shard_map/ppermute | solution.py:72
  108.1 26.2 %collective-permute-start.29 = (bf16[512,256]{1,0:T(8,128)(2,1)S(1)}, bf16[512,256]{1,0:T(8,128)(2,1)S(1)}, u32[]{:S(2)}, u32[]{:S(2)}) collective-permute-start(bf16[512,256]{1,0:T(8,128)(2,1)S(1)} %pad_maximum_fusion.1.refs_8_), channel_id=1, source_target_pairs={{0,16},{8,24},{16,0},{24,8},{1,17},{9,25},{17,1},{25,9},{2,18},{10... | collective-permute-start | bytes 786440 | tf_op jit(solution)/shard_map/ppermute | solution.py:72
  116.3 27.6 %collective-permute-start.30 = (bf16[512,256]{1,0:T(8,128)(2,1)S(1)}, bf16[512,256]{1,0:T(8,128)(2,1)S(1)}, u32[]{:S(2)}, u32[]{:S(2)}) collective-permute-start(bf16[512,256]{1,0:T(8,128)(2,1)S(1)} %pad_maximum_fusion.1.refs_8_), channel_id=1, source_target_pairs={{0,24},{8,16},{16,8},{24,0},{1,25},{9,17},{17,9},{25,1},{2,26},{10... | collective-permute-start | bytes 786440 | tf_op jit(solution)/shard_map/ppermute | solution.py:72
  129.9 20.0 %collective-permute-start.25 = (bf16[144,256]{1,0:T(8,128)(2,1)}, bf16[144,256]{1,0:T(8,128)(2,1)S(1)}, u32[]{:S(2)}, u32[]{:S(2)}) collective-permute-start(bf16[144,256]{1,0:T(8,128)(2,1)} %get-tuple-element.44.refs_0_), channel_id=1, source_target_pairs={{0,8},{8,0},{16,24},{24,16},{1,9},{9,1},{17,25},{25,17},{2,10},{10... | collective-permute-start | bytes 221192 | tf_op jit(solution)/shard_map/ppermute | solution.py:72
  131.9 18.0 %collective-permute-start.26 = (bf16[144,256]{1,0:T(8,128)(2,1)}, bf16[144,256]{1,0:T(8,128)(2,1)S(1)}, u32[]{:S(2)}, u32[]{:S(2)}) collective-permute-start(bf16[144,256]{1,0:T(8,128)(2,1)} %get-tuple-element.44.refs_0_), channel_id=1, source_target_pairs={{0,16},{8,24},{16,0},{24,8},{1,17},{9,25},{17,1},{25,9},{2,18},{10... | collective-permute-start | bytes 221192 | tf_op jit(solution)/shard_map/ppermute | solution.py:72
  133.7 16.2 %collective-permute-start.27 = (bf16[144,256]{1,0:T(8,128)(2,1)}, bf16[144,256]{1,0:T(8,128)(2,1)S(1)}, u32[]{:S(2)}, u32[]{:S(2)}) collective-permute-start(bf16[144,256]{1,0:T(8,128)(2,1)} %get-tuple-element.44.refs_0_), channel_id=1, source_target_pairs={{0,24},{8,16},{16,8},{24,0},{1,25},{9,17},{17,9},{25,1},{2,26},{10... | collective-permute-start | bytes 221192 | tf_op jit(solution)/shard_map/ppermute | solution.py:72
  153.9 10.2 %all-to-all-start = ((bf16[4,256,256]{2,1,0:T(8,128)(2,1)}), bf16[4,256,256]{2,1,0:T(8,128)(2,1)S(1)}, u32[]{:S(2)}, u32[]{:S(2)}) async-start(bf16[4,256,256]{2,1,0:T(8,128)(2,1)} %bitcast.36), calls=%async_computation | async-start | bytes 1048576 | tf_op jit(solution)/shard_map/all_to_all | solution.py:837
  (13 other events, 41.7 us)
